TPU v7x, 256 devices: a whole 4x4x8 slice. The times are simulated.
256 devices in a mesh: ep: 128 (over z, y, x), tp: 2 (over core).
Axes of the slice: x: 4, y: 4, z: 8, core: 2. Of those that a mesh axis runs over, the one named last changes fastest.
Arguments:
- tokens: bfloat16 [2048, 2048], P('ep'), may hold values from -6 to 6
- lengths: int32 [2048], P('ep'), may hold values from 1024 to 8191
- prior_state: float32 [2048, 16, 64, 64], P('ep', 'tp'), may hold values from -2 to 2
- mix_gain: float32 [2048], replicated, may hold values from 0.1 to 1.9
- post_gain: float32 [2048], replicated, may hold values from 0.1 to 1.9
- ffn_gain: float32 [2048], replicated, may hold values from 0.1 to 1.9
- out_gain: float32 [2048], replicated, may hold values from 0.1 to 1.9
- query_weight: bfloat16 [2048, 1024], P('ep', 'tp'), may hold values from -0.125 to 0.125
- key_weight: bfloat16 [2048, 1024], P('ep', 'tp'), may hold values from -0.125 to 0.125
- value_weight: bfloat16 [2048, 1024], P('ep', 'tp'), may hold values from -0.125 to 0.125
- gate_weight: bfloat16 [2048, 1024], P('ep', 'tp'), may hold values from -0.125 to 0.125
- out_weight: bfloat16 [1024, 2048], P('tp', 'ep'), may hold values from -0.1875 to 0.1875
- routes: int32 [2048, 6], P('ep'), may hold values from 0 to 127, all different within a row; in each aligned block of 16 rows (0 to 15, 16 to 31, ...) at most 2 rows name the same one
- route_gates: float32 [2048, 6], P('ep'), may hold values from 0.1 to 0.9
- expert_gate: bfloat16 [128, 2048, 512], P('ep', None, 'tp'), may hold values from -0.125 to 0.125
- expert_up: bfloat16 [128, 2048, 512], P('ep', None, 'tp'), may hold values from -0.125 to 0.125
- expert_down: bfloat16 [128, 512, 2048], P('ep', 'tp'), may hold values from -0.25 to 0.25
- shared_gate: bfloat16 [2048, 512], P(None, 'tp'), may hold values from -0.125 to 0.125
- shared_up: bfloat16 [2048, 512], P(None, 'tp'), may hold values from -0.125 to 0.125
- shared_down: bfloat16 [512, 2048], P('tp'), may hold values from -0.25 to 0.25
Outputs:
- result: bfloat16 [2048, 2048], P('ep')
- new_state: float32 [2048, 16, 64, 64], P('ep', 'tp')
Inputs may be any that keep to these rules, and one draw needn't show every extreme that they name: `routes`: each row names 6 different experts. In the rows of one device (aligned blocks of 16 rows) no expert is named more than 2 times, and in every draw some expert is named exactly 2 times in some block.
All inputs are finite; a program needn't handle non-finite values.
Results may differ from a plain program's by a relative error of at most 0.02.
Values may be sent and summed in bfloat16 or wider, within the bound.
No kernel may reach another device: no remote copies, remote signals or barrier semaphores. Data moves between devices by JAX's collectives and lax.ppermute only.
A program may use at most 128 MiB of HBM per device.

v0:
```python
import jax
import jax.numpy as jnp
from jax import lax
from jax.sharding import Mesh
from jax.sharding import PartitionSpec as P

HEAD = 64
HEADS = 16
Z, Y, X = "ep_0", "ep_1", "ep_2"
EP = (Z, Y, X)


EPS = 1e-06
THETA = 10000.0


def exchanged(blocks, axes):
    return lax.all_to_all(blocks, axes, split_axis=0, concat_axis=0, tiled=True)


def copies(value, count):
    return jnp.broadcast_to(value, (count, *value.shape))


def from_partner(value):
    return lax.ppermute(value, "tp", [(0, 1), (1, 0)])


def rolled_lanes(rows, start):
    doubled = jnp.concatenate([rows, rows], axis=1)
    return lax.dynamic_slice_in_dim(doubled, start, rows.shape[1], 1)


def from_ahead(value, axis, step):
    size = lax.axis_size(axis)
    return lax.ppermute(value, axis, [((i + step) % size, i) for i in range(size)])


def in_place_order(blocks, axis, dim):
    size = blocks.shape[dim]
    doubled = jnp.concatenate([blocks, blocks], axis=dim)
    start = (size - lax.axis_index(axis)) % size
    return lax.dynamic_slice_in_dim(doubled, start, size, dim)


def plane_tokens(by_y):
    size_y, size_x = by_y.shape[0], lax.axis_size(X)
    mine = lax.axis_index(Y)
    column = [lax.dynamic_index_in_dim(by_y, mine, 0, keepdims=False)]
    for step in range(1, size_y):
        behind = (mine - step) % size_y
        block = lax.dynamic_index_in_dim(by_y, behind, 0, keepdims=False)
        column.append(from_ahead(block, Y, step))
    column = in_place_order(jnp.stack(column), Y, 0)
    others = [from_ahead(column, X, step) for step in range(1, size_x)]
    plane = jnp.stack([column, *others])
    return in_place_order(plane, X, 0).swapaxes(0, 1)


def rounded(values):
    return lax.optimization_barrier(values.astype(jnp.bfloat16)).astype(jnp.float32)


def scaled_rows(values, gain_row):
    widened = values.astype(jnp.float32)
    return widened * lax.rsqrt(jnp.mean(widened * widened, axis=-1, keepdims=True) + EPS) * gain_row


def rotate(vectors, lengths):
    half_dim = vectors.shape[-1] // 2
    frequency = THETA ** (-jnp.arange(half_dim, dtype=jnp.float32) / half_dim)
    angles = lengths.astype(jnp.float32)[:, None] * frequency[None, :]
    cosine = jnp.cos(angles)[:, None, :]
    sine_part = jnp.sin(angles)[:, None, :]
    leading = vectors[..., :half_dim]
    trailing = vectors[..., half_dim:]
    return jnp.concatenate(
        [leading * cosine - trailing * sine_part, trailing * cosine + leading * sine_part], axis=-1
    )


def decay_table(head_count):
    head_order = jnp.arange(head_count, dtype=jnp.float32)
    return 1.0 - jnp.exp2(-5.0 - 7.0 * head_order / (head_count - 1))


def retain(queries, keys_new, values, out_gate, prior_state, lengths, decays):
    seq_count = queries.shape[0]
    head_count = decays.shape[0]
    layout = (seq_count, head_count, HEAD)
    rot_query = rotate(queries.astype(jnp.float32).reshape(layout), lengths)
    rot_key = rotate(keys_new.astype(jnp.float32).reshape(layout), lengths) * HEAD ** (-0.5)
    wide_values = values.astype(jnp.float32).reshape(layout)
    from_state = jnp.einsum("shd,shde->she", rot_query, prior_state)
    self_term = jnp.sum(rot_query * rot_key, axis=-1, keepdims=True)
    read_out = decays[None, :, None] * from_state + self_term * wide_values
    normed = read_out * lax.rsqrt(jnp.mean(read_out * read_out, axis=-1, keepdims=True) + EPS)
    gated_rows = normed.reshape(seq_count, head_count * HEAD) * jax.nn.silu(
        out_gate.astype(jnp.float32)
    )
    return (gated_rows.astype(jnp.bfloat16), rot_key, wide_values)


def next_state(decays, prior_state, rot_key, wide_values):
    return (
        decays[None, :, None, None] * prior_state
        + rot_key[..., :, None] * wide_values[..., None, :]
    )


def on_device(
    tokens,
    lengths,
    prior_state,
    mix_gain,
    post_gain,
    ffn_gain,
    out_gain,
    query_weight,
    key_weight,
    value_weight,
    gate_weight,
    out_weight,
    routes,
    route_gates,
    expert_gate,
    expert_up,
    expert_down,
    shared_gate,
    shared_up,
    shared_down,
):
    seq_here, width = tokens.shape
    cols = query_weight.shape[1]
    depth, rows_y, rows_x = (lax.axis_size(axis) for axis in EP)
    experts_all = depth * rows_y * rows_x
    plane = rows_y * rows_x
    core = lax.axis_index("tp")

    kinds = jnp.stack([query_weight, key_weight, value_weight, gate_weight])
    share = cols // rows_x
    wout_parts = out_weight.reshape(rows_x, share, -1).swapaxes(1, 2)
    sent = copies(jnp.concatenate([kinds, wout_parts], axis=2), depth)
    held = exchanged(sent.reshape(depth * rows_x, -1, cols + share), (Z, X))
    held = held.reshape(-1, cols + share)
    kind_weight = held[:, :cols]
    wout_part = held[:, cols:]
    others = [from_ahead(wout_part, X, step) for step in range(1, rows_x)]

    wide_tokens = tokens.astype(jnp.float32)
    gained = (wide_tokens * mix_gain).astype(jnp.bfloat16)
    by_y = gained.reshape(seq_here, depth, rows_y, -1).transpose(2, 0, 1, 3)
    plane_rows = plane_tokens(by_y.reshape(rows_y, seq_here, width // rows_y))
    projected = jnp.dot(
        plane_rows.reshape(plane * seq_here, -1), kind_weight, preferred_element_type=jnp.float32
    ).astype(jnp.bfloat16)
    projected, routes, route_gates = lax.optimization_barrier((projected, routes, route_gates))
    parts = exchanged(projected.reshape(plane, seq_here, cols), (Y, X))
    flat_routes = routes.reshape(-1)
    onehot = (flat_routes[:, None] == jnp.arange(experts_all, dtype=jnp.int32)[None, :]).astype(
        jnp.int32
    )
    earlier = jnp.cumsum(onehot, axis=0) - onehot
    ranks = jnp.sum(earlier * onehot, axis=1)
    mine = jnp.where(ranks == core, flat_routes, -1)
    placing = (jnp.arange(experts_all, dtype=jnp.int32)[:, None] == mine[None, :]).reshape(
        experts_all, seq_here, -1
    )
    dispatch_rows = jnp.any(placing, axis=2).astype(jnp.bfloat16)
    combine = jnp.sum(
        jnp.where(placing, route_gates[None, :, :], jnp.zeros((), jnp.float32)), axis=2
    ).T

    row_scale = lax.rsqrt(jnp.mean(wide_tokens * wide_tokens, axis=-1, keepdims=True) + EPS)

    parts, dispatch_rows, combine, row_scale = lax.optimization_barrier(
        (parts, dispatch_rows, combine, row_scale)
    )
    parts = parts.reshape(rows_y, rows_x, seq_here, cols).astype(jnp.float32)
    queries, keys_new, values, out_gate = (jnp.sum(parts, axis=0) * row_scale).astype(jnp.bfloat16)

    heads_here = cols // HEAD
    decays = lax.dynamic_slice_in_dim(decay_table(HEADS), core * heads_here, heads_here, 0)
    retained, rot_key, wide_values = retain(
        queries, keys_new, values, out_gate, prior_state, lengths, decays
    )

    turned = rolled_lanes(retained, lax.axis_index(X) * share)
    turned, others = lax.optimization_barrier((turned, others))
    wout_turned = jnp.concatenate([wout_part, *others], axis=1)
    retained_y = exchanged(copies(turned, rows_y), Y).reshape(rows_y * seq_here, cols)
    partial_mix = lax.dot_general(
        retained_y, wout_turned, (((1,), (1,)), ((), ())), preferred_element_type=jnp.float32
    ).astype(jnp.bfloat16)
    to_both = partial_mix.reshape(rows_y, 1, seq_here, -1)
    to_both = jnp.broadcast_to(to_both, (rows_y, 2, *to_both.shape[2:]))
    halves = exchanged(to_both.reshape(2 * rows_y, seq_here, -1), (Y, "tp"))
    halves = halves.reshape(rows_y, 2, seq_here, depth, -1).astype(jnp.float32)
    mixed = jnp.sum(halves, axis=1).astype(jnp.bfloat16)
    mixed = mixed.transpose(1, 2, 0, 3).reshape(seq_here, width)
    mixed_sum = rounded(mixed)
    middle = rounded(tokens.astype(jnp.float32) + scaled_rows(mixed_sum, post_gain))
    moe_in = scaled_rows(middle, ffn_gain).astype(jnp.bfloat16)

    outgoing = jnp.dot(dispatch_rows, moe_in, preferred_element_type=jnp.float32).astype(
        jnp.bfloat16
    )
    outgoing, moe_beside, state_beside = lax.optimization_barrier((outgoing, moe_in, prior_state))
    arrived = exchanged(outgoing.reshape(experts_all, 2, -1), EP)

    def lifted(rows, w_gate, w_up):
        return (
            jax.nn.silu(jnp.dot(rows, w_gate, preferred_element_type=jnp.float32))
            * jnp.dot(rows, w_up, preferred_element_type=jnp.float32)
        ).astype(jnp.bfloat16)

    def lowered(rows, w_down):
        return jnp.dot(rows, w_down, preferred_element_type=jnp.float32).astype(jnp.bfloat16)

    new_state = next_state(decays, state_beside, rot_key, wide_values)
    shared_part = lowered(lifted(moe_beside, shared_gate, shared_up), shared_down)
    arrived, shared_part, new_state = lax.optimization_barrier((arrived, shared_part, new_state))

    own_in = arrived.reshape(experts_all, width)
    other_in = from_partner(own_in)
    own_hidden = lifted(own_in, expert_gate[0], expert_up[0])
    own_hidden, other_in = lax.optimization_barrier((own_hidden, other_in))
    other_hidden = lifted(other_in, expert_gate[0], expert_up[0])
    got = from_partner(lowered(other_hidden, expert_down[0]))
    own_sum = lowered(own_hidden, expert_down[0]).astype(jnp.float32) + got.astype(jnp.float32)
    own_sum = own_sum.astype(jnp.bfloat16)
    returned = exchanged(own_sum.reshape(experts_all, 2, -1), EP)
    back_rows = returned.reshape(experts_all, width).astype(jnp.float32)
    mixture_part = jnp.dot(combine, back_rows) + shared_part.astype(jnp.float32)
    mixture = mixture_part + from_partner(mixture_part)
    result = (middle + scaled_rows(mixture, out_gain)).astype(jnp.bfloat16)
    return (result, new_state)


def solution(mesh):
    finer = Mesh(mesh.devices.reshape(-1, 4, 4, mesh.shape["tp"]), ("ep_0", "ep_1", "ep_2", "tp"))
    in_specs = (
        P(EP, None),
        P(EP),
        P(EP, "tp", None, None),
        P(),
        P(),
        P(),
        P(),
        P(EP, "tp"),
        P(EP, "tp"),
        P(EP, "tp"),
        P(EP, "tp"),
        P("tp", EP),
        P(EP, None),
        P(EP, None),
        P(EP, None, "tp"),
        P(EP, None, "tp"),
        P(EP, "tp", None),
        P(None, "tp"),
        P(None, "tp"),
        P("tp", None),
    )
    out_specs = (P(EP, None), P(EP, "tp", None, None))

    return jax.shard_map(
        on_device, mesh=finer, in_specs=in_specs, out_specs=out_specs, check_vma=False
    )
```

profile of v0, /device:TPU:1, one launch (start us, length us, event | category | flops | bytes accessed | tf_op | source)
XLA Modules:
  0.0 147.3 jit_solution(8287600717978557673)
XLA Ops:
  0.7 1.0 fusion.28
  1.8 0.2 reshape.225
  2.0 0.1 reshape.226
  2.2 2.2 %collective-permute-start.2 = (bf16[16,512]{1,0:T(8,128)(2,1)S(1)}, bf16[16,512]{1,0:T(8,128)(2,1)S(1)}, u32[]{:S(2)}, u32[]{:S(2)}) collective-permute-start(bf16[16,512]{1,0:T(8,128)(2,1)S(1)} %get-tuple-element.53), channel_id=1, source_target_pairs={{24,0},{0,8},{8,16},{16,24},{25,1},{1,9},{9,17},{17,25},{26,2},{2,... | collective-permute-start | bytes 49160 | tf_op jit(solution)/shard_map/ppermute | solution.py:36
  4.4 2.6 %collective-permute-start.1 = (bf16[16,512]{1,0:T(8,128)(2,1)S(1)}, bf16[16,512]{1,0:T(8,128)(2,1)S(1)}, u32[]{:S(2)}, u32[]{:S(2)}) collective-permute-start(bf16[16,512]{1,0:T(8,128)(2,1)S(1)} %get-tuple-element.55), channel_id=1, source_target_pairs={{16,0},{24,8},{0,16},{8,24},{17,1},{25,9},{1,17},{9,25},{18,2},{26... | collective-permute-start | bytes 49160 | tf_op jit(solution)/shard_map/ppermute | solution.py:36
  7.0 1.1 collective-permute-start
  8.1 0.7 bitcast_bitcast_fusion
  8.8 0.8 pad_maximum_fusion
  9.6 0.9 broadcast_in_dim.24
  10.4 11.0 %all-to-all-start = ((bf16[32,16,640]{2,1,0:T(8,128)(2,1)}), bf16[32,16,640]{2,1,0:T(8,128)(2,1)S(1)}, u32[]{:S(2)}, u32[]{:S(2)}) async-start(bf16[32,16,640]{2,1,0:T(8,128)(2,1)} %bitcast.18), calls=%async_computation | async-start | bytes 1310720 | tf_op jit(solution)/shard_map/all_to_all | solution.py:18
  21.5 0.7 convert_element_type.127
  22.2 0.1 multiply_cosine_fusion
  22.5 2.5 %collective-permute-start.3 = (bf16[4,16,512]{2,1,0:T(8,128)(2,1)S(1)}, bf16[4,16,512]{2,1,0:T(8,128)(2,1)S(1)}, u32[]{:S(2)}, u32[]{:S(2)}) collective-permute-start(bf16[4,16,512]{2,1,0:T(8,128)(2,1)S(1)} %get-tuple-element.43), channel_id=1, source_target_pairs={{2,0},{4,2},{6,4},{0,6},{3,1},{5,3},{7,5},{1,7},{10,8},{12,10},{14... | collective-permute-start | bytes 196616 | tf_op jit(solution)/shard_map/ppermute | solution.py:36
  25.1 1.7 %collective-permute-start.4 = (bf16[4,16,512]{2,1,0:T(8,128)(2,1)S(1)}, bf16[4,16,512]{2,1,0:T(8,128)(2,1)S(1)}, u32[]{:S(2)}, u32[]{:S(2)}) collective-permute-start(bf16[4,16,512]{2,1,0:T(8,128)(2,1)S(1)} %get-tuple-element.43), channel_id=1, source_target_pairs={{4,0},{6,2},{0,4},{2,6},{5,1},{7,3},{1,5},{3,7},{12,8},{14,10},{8,... | collective-permute-start | bytes 196616 | tf_op jit(solution)/shard_map/ppermute | solution.py:36
  26.9 0.4 collective-permute-done.3
  27.3 3.5 %collective-permute-done.4 = bf16[4,16,512]{2,1,0:T(8,128)(2,1)S(1)} collective-permute-done((bf16[4,16,512]{2,1,0:T(8,128)(2,1)S(1)}, bf16[4,16,512]{2,1,0:T(8,128)(2,1)S(1)}, u32[]{:S(2)}, u32[]{:S(2)}) %collective-permute-start.4) | collective-permute-done | bytes 65568 | tf_op jit(solution)/shard_map/ppermute | solution.py:36
  30.8 0.7 collective-permute-done.5
  31.6 7.5 %all-to-all-done = bf16[32,16,640]{2,1,0:T(8,128)(2,1)S(1)} async-done(((bf16[32,16,640]{2,1,0:T(8,128)(2,1)}), bf16[32,16,640]{2,1,0:T(8,128)(2,1)S(1)}, u32[]{:S(2)}, u32[]{:S(2)}) %all-to-all-start) | async-done | bytes 655392 | tf_op jit(solution)/shard_map/all_to_all | solution.py:18
  39.1 1.7 %collective-permute-start.8 = (bf16[512,128]{1,0:T(8,128)(2,1)S(1)}, bf16[512,128]{1,0:T(8,128)(2,1)S(1)}, u32[]{:S(2)}, u32[]{:S(2)}) collective-permute-start(bf16[512,128]{1,0:T(8,128)(2,1)S(1)} %slice.29), channel_id=1, source_target_pairs={{6,0},{0,2},{2,4},{4,6},{7,1},{1,3},{3,5},{5,7},{14,8},{8,10},{10,... | collective-permute-start | bytes 393224 | tf_op jit(solution)/shard_map/ppermute | solution.py:36
  40.8 1.9 %collective-permute-start.7 = (bf16[512,128]{1,0:T(8,128)(2,1)S(1)}, bf16[512,128]{1,0:T(8,128)(2,1)S(1)}, u32[]{:S(2)}, u32[]{:S(2)}) collective-permute-start(bf16[512,128]{1,0:T(8,128)(2,1)S(1)} %slice.29), channel_id=1, source_target_pairs={{4,0},{6,2},{0,4},{2,6},{5,1},{7,3},{1,5},{3,7},{12,8},{14,10},{8,... | collective-permute-start | bytes 393224 | tf_op jit(solution)/shard_map/ppermute | solution.py:36
  42.6 2.0 %collective-permute-start.6 = (bf16[512,128]{1,0:T(8,128)(2,1)S(1)}, bf16[512,128]{1,0:T(8,128)(2,1)S(1)}, u32[]{:S(2)}, u32[]{:S(2)}) collective-permute-start(bf16[512,128]{1,0:T(8,128)(2,1)S(1)} %slice.29), channel_id=1, source_target_pairs={{2,0},{4,2},{6,4},{0,6},{3,1},{5,3},{7,5},{1,7},{10,8},{12,10},{14... | collective-permute-start | bytes 393224 | tf_op jit(solution)/shard_map/ppermute | solution.py:36
  44.6 1.0 convolution_convert_fusion.4
  45.8 3.5 %all-to-all-start.1 = ((bf16[16,16,512]{2,1,0:T(8,128)(2,1)}), bf16[16,16,512]{2,1,0:T(8,128)(2,1)S(1)}, u32[]{:S(2)}, u32[]{:S(2)}) async-start(bf16[16,16,512]{2,1,0:T(8,128)(2,1)} %bitcast.20), calls=%async_computation.1 | async-start | bytes 524288 | tf_op jit(solution)/shard_map/all_to_all | solution.py:18
  49.4 0.1 reduce_window_sum.11
  49.5 0.2 select_reduce_fusion.1
  49.9 0.1 fusion.40
  50.1 6.7 %all-to-all-done.1 = bf16[16,16,512]{2,1,0:T(8,128)(2,1)S(1)} async-done(((bf16[16,16,512]{2,1,0:T(8,128)(2,1)}), bf16[16,16,512]{2,1,0:T(8,128)(2,1)S(1)}, u32[]{:S(2)}, u32[]{:S(2)}) %all-to-all-start.1) | async-done | bytes 262176 | tf_op jit(solution)/shard_map/all_to_all | solution.py:18
  57.2 0.1 multiply_subtract_fusion
  57.3 0.1 pad_maximum_fusion.1
  57.4 2.9 %fusion.57 = f32[16,8,1,64]{3,2,1,0:T(1,128)S(1)} fusion(f32[16,8,64,1]{2,3,1,0:T(1,128)S(1)} %bitcast.119, f32[16,8,64,64]{3,2,1,0:T(8,128)} %param.22), kind=kOutput, calls=%fused_computation.131 | convolution fusion | flops 1048576 | bytes 2162688 | tf_op jit(solution)/shard_map/shd,shde->she/dot_general | solution.py:94
  60.3 0.2 multiply_reduce_fusion.1
  60.8 6.8 %all_to_all.30 = bf16[4,16,512]{2,1,0:T(8,128)(2,1)S(1)} all-to-all(bf16[4,16,512]{2,1,0:T(8,128)(2,1)S(1)} %broadcast_in_dim.28), channel_id=1, replica_groups=mesh['ep_0'=8,'ep_1'=4,'ep_2'=4,'tp'=2] {'ep_1'}, dimensions={0} | all-to-all | bytes 131072 | tf_op jit(solution)/shard_map/all_to_all | solution.py:18
  67.7 0.3 convolution_convert_fusion.5
  68.0 13.4 %all_to_all.31 = bf16[8,16,512]{2,1,0:T(8,128)(2,1)S(1)} all-to-all(bf16[8,16,512]{2,1,0:T(8,128)(2,1)S(1)} %bitcast.122), channel_id=1, replica_groups=mesh['ep_0'=8,'ep_1'=4,'ep_2'=4,'tp'=2] {'ep_1','tp'}, dimensions={0} | all-to-all | bytes 262144 | tf_op jit(solution)/shard_map/all_to_all | solution.py:18
  81.4 0.2 reshape.235
  81.7 0.1 copy.38
  81.8 0.2 reshape.236
  82.0 0.1 fusion.25
  82.1 0.1 fusion.29
  82.2 0.1 fusion.30
  82.5 0.3 convolution_convert_fusion.2
  82.8 1.2 reshape.237
  83.9 6.3 %all-to-all-start.4 = ((bf16[128,2,1024]{2,1,0:T(2,128)(2,1)}), bf16[128,2,1024]{2,1,0:T(2,128)(2,1)S(1)}, u32[]{:S(2)}, u32[]{:S(2)}) async-start(bf16[128,2,1024]{2,1,0:T(2,128)(2,1)} %reshape.237), calls=%async_computation.4 | async-start | bytes 1048576 | tf_op jit(solution)/shard_map/all_to_all | solution.py:18
  90.3 1.5 fusion.58
  91.8 2.3 %convolution_convert_fusion.3 = bf16[16,2048]{1,0:T(8,128)(2,1)S(1)} fusion(bf16[256,2048]{1,0:T(8,128)(2,1)} %param.39, bf16[16,2048]{1,0:T(8,128)(2,1)S(1)} %fusion.32, bf16[2048,256]{1,0:T(8,128)(2,1)} %param.38, f32[16,256]{1,0:T(8,128)S(1)} %fusion.58), kind=kOutput, calls=%fused_computation.9 | convolution fusion | flops 33611776 | bytes 2244608 | tf_op jit(solution)/shard_map/dot_general | solution.py:218
  94.0 4.4 %multiply_add_fusion = f32[16,8,64,64]{3,2,1,0:T(8,128)} fusion(f32[16,8,64,64]{3,2,1,0:T(8,128)} %param.22, f32[16,8,64]{2,1,0:T(8,128)S(1)} %reshape.244, f32[16,8,64]{2,1,0:T(8,128)S(1)} %get-tuple-element.64, f32[8]{0:T(128)S(1)} %dynamic_slice.25), kind=kLoop, calls=%fused_computation.1 | loop fusion | flops 1572864 | bytes 4259872 | tf_op jit(solution)/shard_map/add | solution.py:106
  98.4 10.5 %all-to-all-done.4 = bf16[128,2,1024]{2,1,0:T(2,128)(2,1)S(1)} async-done(((bf16[128,2,1024]{2,1,0:T(2,128)(2,1)}), bf16[128,2,1024]{2,1,0:T(2,128)(2,1)S(1)}, u32[]{:S(2)}, u32[]{:S(2)}) %all-to-all-start.4) | async-done | bytes 524320 | tf_op jit(solution)/shard_map/all_to_all | solution.py:18
  109.0 0.1 copy.42
  109.1 3.1 %collective-permute-start.9 = (bf16[128,2048]{1,0:T(8,128)(2,1)S(1)}, bf16[128,2048]{1,0:T(8,128)(2,1)S(1)}, u32[]{:S(2)}, u32[]{:S(2)}) collective-permute-start(bf16[128,2048]{1,0:T(8,128)(2,1)S(1)} %bitcast.111), channel_id=1, source_target_pairs={{0,1},{1,0},{2,3},{3,2},{4,5},{5,4},{6,7},{7,6},{8,9},{9,8},{10,11... | collective-permute-start | bytes 1572872 | tf_op jit(solution)/shard_map/ppermute | solution.py:26
  112.2 0.3 fusion.15
  112.5 1.5 %fusion.4 = bf16[128,256]{1,0:T(8,128)(2,1)S(1)} fusion(bf16[128,2048]{1,0:T(8,128)(2,1)S(1)} %bitcast.113, bf16[1,2048,256]{2,1,0:T(8,128)(2,1)} %param.35, f32[128,256]{1,0:T(8,128)S(1)} %fusion.15), kind=kOutput, calls=%fused_computation.12 | convolution fusion | flops 134414336 | bytes 1769472 | tf_op jit(solution)/shard_map/dot_general | solution.py:214
  114.1 0.3 fusion.10
  114.4 0.8 convolution_convert_fusion
  115.2 0.1 collective-permute-start.10
  115.3 1.9 %collective-permute-done.10 = bf16[128,2048]{1,0:T(8,128)(2,1)S(1)} collective-permute-done((bf16[128,2048]{1,0:T(8,128)(2,1)S(1)}, bf16[128,2048]{1,0:T(8,128)(2,1)S(1)}, u32[]{:S(2)}, u32[]{:S(2)}) %collective-permute-start.10) | collective-permute-done | bytes 524320 | tf_op jit(solution)/shard_map/ppermute | solution.py:26
  117.2 0.3 fusion.3
  117.5 0.4 reshape.239
  117.9 24.9 %all_to_all.32 = bf16[128,2,1024]{2,1,0:T(2,128)(2,1)S(1)} all-to-all(bf16[128,2,1024]{2,1,0:T(2,128)(2,1)S(1)} %reshape.239), channel_id=1, replica_groups=mesh['ep_0'=8,'ep_1'=4,'ep_2'=4,'tp'=2] {'ep_0','ep_1','ep_2'}, dimensions={0} | all-to-all | bytes 1048576 | tf_op jit(solution)/shard_map/all_to_all | solution.py:18
  142.8 0.1 copy.43
  142.9 0.2 convolution_add_fusion
  143.1 2.3 %collective-permute-start.11 = (f32[16,2048]{1,0:T(8,128)S(1)}, f32[16,2048]{1,0:T(8,128)S(1)}, u32[]{:S(2)}, u32[]{:S(2)}) collective-permute-start(f32[16,2048]{1,0:T(8,128)S(1)} %convolution_add_fusion), channel_id=1, source_target_pairs={{0,1},{1,0},{2,3},{3,2},{4,5},{5,4},{6,7},{7,6},{8,9},{9,8},{10,11... | collective-permute-start | bytes 393224 | tf_op jit(solution)/shard_map/ppermute | solution.py:26
  145.5 1.0 collective-permute-done.11
  146.4 0.1 multiply_reduce_fusion
  146.6 0.7 fusion.33
  (77 shorter events, 1.7 us)
Async XLA Ops:
  0.6 113.8 %copy-start = (bf16[1,256,2048]{2,1,0:T(8,128)(2,1)S(1)}, bf16[1,256,2048]{2,1,0:T(8,128)(2,1)}, u32[]{:S(2)}) copy-start(bf16[1,256,2048]{2,1,0:T(8,128)(2,1)} %param.36) | copy-start | bytes 3145732
  0.6 49.4 %copy-start.8 = (f32[16,6]{0,1:T(8,128)S(1)}, f32[16,6]{0,1:T(8,128)}, u32[]{:S(2)}) copy-start(f32[16,6]{0,1:T(8,128)} %param.33) | copy-start | bytes 1156
  0.7 44.9 %copy-start.7 = (s32[16,6]{0,1:T(8,128)S(1)}, s32[16,6]{0,1:T(8,128)}, u32[]{:S(2)}) copy-start(s32[16,6]{0,1:T(8,128)} %param.32) | copy-start | bytes 1156
  2.2 20.2 %collective-permute-start.2 = (bf16[16,512]{1,0:T(8,128)(2,1)S(1)}, bf16[16,512]{1,0:T(8,128)(2,1)S(1)}, u32[]{:S(2)}, u32[]{:S(2)}) collective-permute-start(bf16[16,512]{1,0:T(8,128)(2,1)S(1)} %get-tuple-element.53), channel_id=1, source_target_pairs={{24,0},{0,8},{8,16},{16,24},{25,1},{1,9},{9,17},{17,25},{26,2},{2,... | collective-permute-start | bytes 49160 | tf_op jit(solution)/shard_map/ppermute | solution.py:36
  4.4 18.0 %collective-permute-start.1 = (bf16[16,512]{1,0:T(8,128)(2,1)S(1)}, bf16[16,512]{1,0:T(8,128)(2,1)S(1)}, u32[]{:S(2)}, u32[]{:S(2)}) collective-permute-start(bf16[16,512]{1,0:T(8,128)(2,1)S(1)} %get-tuple-element.55), channel_id=1, source_target_pairs={{16,0},{24,8},{0,16},{8,24},{17,1},{25,9},{1,17},{9,25},{18,2},{26... | collective-permute-start | bytes 49160 | tf_op jit(solution)/shard_map/ppermute | solution.py:36
  7.0 15.4 %collective-permute-start = (bf16[16,512]{1,0:T(8,128)(2,1)S(1)}, bf16[16,512]{1,0:T(8,128)(2,1)S(1)}, u32[]{:S(2)}, u32[]{:S(2)}) collective-permute-start(bf16[16,512]{1,0:T(8,128)(2,1)S(1)} %get-tuple-element.56), channel_id=1, source_target_pairs={{8,0},{16,8},{24,16},{0,24},{9,1},{17,9},{25,17},{1,25},{10,2},{18... | collective-permute-start | bytes 49160 | tf_op jit(solution)/shard_map/ppermute | solution.py:36
  10.4 28.6 %all-to-all-start = ((bf16[32,16,640]{2,1,0:T(8,128)(2,1)}), bf16[32,16,640]{2,1,0:T(8,128)(2,1)S(1)}, u32[]{:S(2)}, u32[]{:S(2)}) async-start(bf16[32,16,640]{2,1,0:T(8,128)(2,1)} %bitcast.18), calls=%async_computation | async-start | bytes 1310720 | tf_op jit(solution)/shard_map/all_to_all | solution.py:18
  22.5 4.8 %collective-permute-start.3 = (bf16[4,16,512]{2,1,0:T(8,128)(2,1)S(1)}, bf16[4,16,512]{2,1,0:T(8,128)(2,1)S(1)}, u32[]{:S(2)}, u32[]{:S(2)}) collective-permute-start(bf16[4,16,512]{2,1,0:T(8,128)(2,1)S(1)} %get-tuple-element.43), channel_id=1, source_target_pairs={{2,0},{4,2},{6,4},{0,6},{3,1},{5,3},{7,5},{1,7},{10,8},{12,10},{14... | collective-permute-start | bytes 196616 | tf_op jit(solution)/shard_map/ppermute | solution.py:36
  25.1 6.4 %collective-permute-start.5 = (bf16[4,16,512]{2,1,0:T(8,128)(2,1)S(1)}, bf16[4,16,512]{2,1,0:T(8,128)(2,1)S(1)}, u32[]{:S(2)}, u32[]{:S(2)}) collective-permute-start(bf16[4,16,512]{2,1,0:T(8,128)(2,1)S(1)} %get-tuple-element.43), channel_id=1, source_target_pairs={{6,0},{0,2},{2,4},{4,6},{7,1},{1,3},{3,5},{5,7},{14,8},{8,10},{10,... | collective-permute-start | bytes 196616 | tf_op jit(solution)/shard_map/ppermute | solution.py:36
  25.1 5.7 %collective-permute-start.4 = (bf16[4,16,512]{2,1,0:T(8,128)(2,1)S(1)}, bf16[4,16,512]{2,1,0:T(8,128)(2,1)S(1)}, u32[]{:S(2)}, u32[]{:S(2)}) collective-permute-start(bf16[4,16,512]{2,1,0:T(8,128)(2,1)S(1)} %get-tuple-element.43), channel_id=1, source_target_pairs={{4,0},{6,2},{0,4},{2,6},{5,1},{7,3},{1,5},{3,7},{12,8},{14,10},{8,... | collective-permute-start | bytes 196616 | tf_op jit(solution)/shard_map/ppermute | solution.py:36
  39.1 21.7 %collective-permute-start.8 = (bf16[512,128]{1,0:T(8,128)(2,1)S(1)}, bf16[512,128]{1,0:T(8,128)(2,1)S(1)}, u32[]{:S(2)}, u32[]{:S(2)}) collective-permute-start(bf16[512,128]{1,0:T(8,128)(2,1)S(1)} %slice.29), channel_id=1, source_target_pairs={{6,0},{0,2},{2,4},{4,6},{7,1},{1,3},{3,5},{5,7},{14,8},{8,10},{10,... | collective-permute-start | bytes 393224 | tf_op jit(solution)/shard_map/ppermute | solution.py:36
  40.8 20.0 %collective-permute-start.7 = (bf16[512,128]{1,0:T(8,128)(2,1)S(1)}, bf16[512,128]{1,0:T(8,128)(2,1)S(1)}, u32[]{:S(2)}, u32[]{:S(2)}) collective-permute-start(bf16[512,128]{1,0:T(8,128)(2,1)S(1)} %slice.29), channel_id=1, source_target_pairs={{4,0},{6,2},{0,4},{2,6},{5,1},{7,3},{1,5},{3,7},{12,8},{14,10},{8,... | collective-permute-start | bytes 393224 | tf_op jit(solution)/shard_map/ppermute | solution.py:36
  42.6 18.2 %collective-permute-start.6 = (bf16[512,128]{1,0:T(8,128)(2,1)S(1)}, bf16[512,128]{1,0:T(8,128)(2,1)S(1)}, u32[]{:S(2)}, u32[]{:S(2)}) collective-permute-start(bf16[512,128]{1,0:T(8,128)(2,1)S(1)} %slice.29), channel_id=1, source_target_pairs={{2,0},{4,2},{6,4},{0,6},{3,1},{5,3},{7,5},{1,7},{10,8},{12,10},{14... | collective-permute-start | bytes 393224 | tf_op jit(solution)/shard_map/ppermute | solution.py:36
  45.8 11.1 %all-to-all-start.1 = ((bf16[16,16,512]{2,1,0:T(8,128)(2,1)}), bf16[16,16,512]{2,1,0:T(8,128)(2,1)S(1)}, u32[]{:S(2)}, u32[]{:S(2)}) async-start(bf16[16,16,512]{2,1,0:T(8,128)(2,1)} %bitcast.20), calls=%async_computation.1 | async-start | bytes 524288 | tf_op jit(solution)/shard_map/all_to_all | solution.py:18
  57.4 24.7 %copy-start.3 = (bf16[16,2048]{1,0:T(8,128)(2,1)S(1)}, bf16[16,2048]{1,0:T(8,128)(2,1)}, u32[]{:S(2)}) copy-start(bf16[16,2048]{1,0:T(8,128)(2,1)} %param.20) | copy-start | bytes 196612
  57.4 24.7 %copy-start.4 = (f32[2048]{0:T(1024)S(1)}, f32[2048]{0:T(1024)}, u32[]{:S(2)}) copy-start(f32[2048]{0:T(1024)} %param.24) | copy-start | bytes 24580
  57.4 24.9 %copy-start.5 = (f32[2048]{0:T(1024)S(1)}, f32[2048]{0:T(1024)}, u32[]{:S(2)}) copy-start(f32[2048]{0:T(1024)} %param.25) | copy-start | bytes 24580
  83.9 25.0 %all-to-all-start.4 = ((bf16[128,2,1024]{2,1,0:T(2,128)(2,1)}), bf16[128,2,1024]{2,1,0:T(2,128)(2,1)S(1)}, u32[]{:S(2)}, u32[]{:S(2)}) async-start(bf16[128,2,1024]{2,1,0:T(2,128)(2,1)} %reshape.237), calls=%async_computation.4 | async-start | bytes 1048576 | tf_op jit(solution)/shard_map/all_to_all | solution.py:18
  94.0 18.1 %copy-start.1 = (bf16[1,2048,256]{2,1,0:T(8,128)(2,1)S(1)}, bf16[1,2048,256]{2,1,0:T(8,128)(2,1)}, u32[]{:S(2)}) copy-start(bf16[1,2048,256]{2,1,0:T(8,128)(2,1)} %param.34) | copy-start | bytes 3145732
  109.0 5.1 %copy-start.2 = (bf16[1,2048,256]{2,1,0:T(8,128)(2,1)S(1)}, bf16[1,2048,256]{2,1,0:T(8,128)(2,1)}, u32[]{:S(2)}) copy-start(bf16[1,2048,256]{2,1,0:T(8,128)(2,1)} %param.35) | copy-start | bytes 3145732
  109.1 5.0 %collective-permute-start.9 = (bf16[128,2048]{1,0:T(8,128)(2,1)S(1)}, bf16[128,2048]{1,0:T(8,128)(2,1)S(1)}, u32[]{:S(2)}, u32[]{:S(2)}) collective-permute-start(bf16[128,2048]{1,0:T(8,128)(2,1)S(1)} %bitcast.111), channel_id=1, source_target_pairs={{0,1},{1,0},{2,3},{3,2},{4,5},{5,4},{6,7},{7,6},{8,9},{9,8},{10,11... | collective-permute-start | bytes 1572872 | tf_op jit(solution)/shard_map/ppermute | solution.py:26
  114.4 32.2 %copy-start.6 = (f32[2048]{0:T(1024)S(1)}, f32[2048]{0:T(1024)}, u32[]{:S(2)}) copy-start(f32[2048]{0:T(1024)} %param.26) | copy-start | bytes 24580
  115.2 2.0 %collective-permute-start.10 = (bf16[128,2048]{1,0:T(8,128)(2,1)S(1)}, bf16[128,2048]{1,0:T(8,128)(2,1)S(1)}, u32[]{:S(2)}, u32[]{:S(2)}) collective-permute-start(bf16[128,2048]{1,0:T(8,128)(2,1)S(1)} %convolution_convert_fusion), channel_id=1, source_target_pairs={{0,1},{1,0},{2,3},{3,2},{4,5},{5,4},{6,7},{7,6},{8,9},{9,8},{10,11... | collective-permute-start | bytes 1572872 | tf_op jit(solution)/shard_map/ppermute | solution.py:26
  143.1 3.3 %collective-permute-start.11 = (f32[16,2048]{1,0:T(8,128)S(1)}, f32[16,2048]{1,0:T(8,128)S(1)}, u32[]{:S(2)}, u32[]{:S(2)}) collective-permute-start(f32[16,2048]{1,0:T(8,128)S(1)} %convolution_add_fusion), channel_id=1, source_target_pairs={{0,1},{1,0},{2,3},{3,2},{4,5},{5,4},{6,7},{7,6},{8,9},{9,8},{10,11... | collective-permute-start | bytes 393224 | tf_op jit(solution)/shard_map/ppermute | solution.py:26
where the time goes:
time: 148 us; the launch traced here: 147 us
  blocking collectives  45.2 us (31%)
  starting transfers between devices  42.1 us (28%)
  waiting for transfers between devices  32.2 us (22%)
  matrix products  11.7 us (8%)
  other arithmetic  9.66 us (7%)
  local copies, waits for them, and re-layouts  5.15 us (3%)
    all_to_all x3, blocking collectives, exchanged(): return lax.all_to_all(blocks, axes, split_axis=0, concat_axis=0, tiled=True)  45.2 us
    all_to_all x3, waiting for transfers between devices, exchanged(): return lax.all_to_all(blocks, axes, split_axis=0, concat_axis=0, tiled=True)  24.7 us
    all_to_all x3, starting transfers between devices, exchanged(): return lax.all_to_all(blocks, axes, split_axis=0, concat_axis=0, tiled=True)  20.9 us
    ppermute x9, starting transfers between devices, from_ahead(): lax.ppermute(value, axis, [((i + step) % size, i) for i in range(size)])  15.6 us
    ppermute x3, starting transfers between devices, from_partner(): return lax.ppermute(value, 'tp', [(0, 1), (1, 0)])  5.53 us
    ppermute x9, waiting for transfers between devices, from_ahead(): lax.ppermute(value, axis, [((i + step) % size, i) for i in range(size)])  4.65 us
    add x1, other arithmetic, next_state(): decays[None, :, None, None] * prior_state  4.37 us
    dot_general x3, matrix products, lowered(): jnp.dot(rows, w_down, preferred_element_type=jnp.float32)  3.37 us
  transfers between devices with their start and end apart: 15, of which 8 were waited for; matrix products, arithmetic and copies ran while one was open for 13% of the time, Pallas kernels for 0%

commit v1 on v0

--- a/solution.py
+++ b/solution.py
@@ -1,6 +1,8 @@
 import jax
 import jax.numpy as jnp
 from jax import lax
+from jax.experimental import pallas as pl
+from jax.experimental.pallas import tpu as pltpu
 from jax.sharding import Mesh
 from jax.sharding import PartitionSpec as P
 
@@ -106,6 +108,41 @@
         decays[None, :, None, None] * prior_state
         + rot_key[..., :, None] * wide_values[..., None, :]
     )
+
+
+def expert_body(rows, gate_a, up_a, down_a, gate_b, up_b, down_b, out, total):
+    step = pl.program_id(0)
+
+    @pl.when(step == 0)
+    def _():
+        total[...] = jnp.zeros_like(total)
+
+    for gate, up, down in ((gate_a, up_a, down_a), (gate_b, up_b, down_b)):
+        gated = jnp.dot(rows[...], gate[...], preferred_element_type=jnp.float32)
+        lifted = jnp.dot(rows[...], up[...], preferred_element_type=jnp.float32)
+        hidden = (jax.nn.silu(gated) * lifted).astype(jnp.bfloat16)
+        total[...] += jnp.dot(hidden, down[...], preferred_element_type=jnp.float32)
+
+    @pl.when(step == pl.num_programs(0) - 1)
+    def _():
+        out[...] = total[...].astype(jnp.bfloat16)
+
+
+def whole_expert(rows, here, there):
+    count, width = rows.shape
+    units, block = here[0].shape[1], 128
+    across = pl.BlockSpec((width, block), lambda i: (0, i))
+    down = pl.BlockSpec((block, width), lambda i: (i, 0))
+    whole = pl.BlockSpec((count, width), lambda i: (0, 0))
+    return pl.pallas_call(
+        expert_body,
+        grid=(units // block,),
+        in_specs=[whole, across, across, down, across, across, down],
+        out_specs=whole,
+        out_shape=jax.ShapeDtypeStruct((count, width), jnp.bfloat16),
+        scratch_shapes=[pltpu.VMEM((count, width), jnp.float32)],
+        compiler_params=pltpu.CompilerParams(dimension_semantics=("arbitrary",)),
+    )(rows, *here, *there)
 
 
 def on_device(
@@ -154,7 +191,9 @@
     projected = jnp.dot(
         plane_rows.reshape(plane * seq_here, -1), kind_weight, preferred_element_type=jnp.float32
     ).astype(jnp.bfloat16)
-    projected, routes, route_gates = lax.optimization_barrier((projected, routes, route_gates))
+    projected, routes, route_gates, lengths = lax.optimization_barrier(
+        (projected, routes, route_gates, lengths)
+    )
     parts = exchanged(projected.reshape(plane, seq_here, cols), (Y, X))
     flat_routes = routes.reshape(-1)
     onehot = (flat_routes[:, None] == jnp.arange(experts_all, dtype=jnp.int32)[None, :]).astype(
@@ -205,30 +244,25 @@
     outgoing = jnp.dot(dispatch_rows, moe_in, preferred_element_type=jnp.float32).astype(
         jnp.bfloat16
     )
-    outgoing, moe_beside, state_beside = lax.optimization_barrier((outgoing, moe_in, prior_state))
+    expert_here = (expert_gate[0], expert_up[0], expert_down[0])
+    outgoing, moe_beside, prior_state, expert_here = lax.optimization_barrier(
+        (outgoing, moe_in, prior_state, expert_here)
+    )
     arrived = exchanged(outgoing.reshape(experts_all, 2, -1), EP)
 
-    def lifted(rows, w_gate, w_up):
-        return (
-            jax.nn.silu(jnp.dot(rows, w_gate, preferred_element_type=jnp.float32))
-            * jnp.dot(rows, w_up, preferred_element_type=jnp.float32)
-        ).astype(jnp.bfloat16)
-
-    def lowered(rows, w_down):
-        return jnp.dot(rows, w_down, preferred_element_type=jnp.float32).astype(jnp.bfloat16)
-
-    new_state = next_state(decays, state_beside, rot_key, wide_values)
-    shared_part = lowered(lifted(moe_beside, shared_gate, shared_up), shared_down)
-    arrived, shared_part, new_state = lax.optimization_barrier((arrived, shared_part, new_state))
-
-    own_in = arrived.reshape(experts_all, width)
-    other_in = from_partner(own_in)
-    own_hidden = lifted(own_in, expert_gate[0], expert_up[0])
-    own_hidden, other_in = lax.optimization_barrier((own_hidden, other_in))
-    other_hidden = lifted(other_in, expert_gate[0], expert_up[0])
-    got = from_partner(lowered(other_hidden, expert_down[0]))
-    own_sum = lowered(own_hidden, expert_down[0]).astype(jnp.float32) + got.astype(jnp.float32)
-    own_sum = own_sum.astype(jnp.bfloat16)
+    expert_there = tuple(from_partner(weight) for weight in expert_here)
+    new_state = next_state(decays, prior_state, rot_key, wide_values)
+    shared_gated = jnp.dot(moe_beside, shared_gate, preferred_element_type=jnp.float32)
+    shared_lifted = jnp.dot(moe_beside, shared_up, preferred_element_type=jnp.float32)
+    shared_hidden = (jax.nn.silu(shared_gated) * shared_lifted).astype(jnp.bfloat16)
+    shared_part = jnp.dot(shared_hidden, shared_down, preferred_element_type=jnp.float32).astype(
+        jnp.bfloat16
+    )
+    arrived, shared_part, new_state, expert_there = lax.optimization_barrier(
+        (arrived, shared_part, new_state, expert_there)
+    )
+
+    own_sum = whole_expert(arrived.reshape(experts_all, width), expert_here, expert_there)
     returned = exchanged(own_sum.reshape(experts_all, 2, -1), EP)
     back_rows = returned.reshape(experts_all, width).astype(jnp.float32)
     mixture_part = jnp.dot(combine, back_rows) + shared_part.astype(jnp.float32)

time: 148 us -> 150 us (1.014)
  Pallas kernels: 0 us -> 5.79 us
  matrix products: 11.7 us -> 8.14 us
  local copies, waits for them, and re-layouts: 5.15 us -> 6.99 us
    pallas_call x0 -> x1, Pallas kernels: none -> 5.79 us  [whole_expert(): pl.pallas_call(expert_body, grid=(units // block,), in_specs=[whole, acro...]
    dot_general x7 -> x2, matrix products: 7.02 us -> 3.42 us  [the longest x1 1.95 us: on_device(): jnp.dot(shared_hidden, shared_down, preferred_element_type=jnp.float32)]
    ppermute x3 -> x4, waiting for transfers between devices: 2.88 us -> 0.99 us  [from_partner(): return lax.ppermute(value, 'tp', [(0, 1), (1, 0)])]
    ppermute x3 -> x4, starting transfers between devices: 5.53 us -> 5.4 us  [from_partner(): return lax.ppermute(value, 'tp', [(0, 1), (1, 0)])]
  transfers between devices with their start and end apart: 15 -> 16, of which waited for: 8 -> 6; matrix products, arithmetic and copies ran while one was open for 13% -> 12% of each run, Pallas kernels for 0% -> 0%
where the time goes in v1:
time: 150 us; the launch traced here: 149 us
  blocking collectives  44.2 us (29%)
  starting transfers between devices  41.8 us (28%)
  waiting for transfers between devices  32.1 us (21%)
  other arithmetic  8.93 us (6%)
  matrix products  8.14 us (5%)
  local copies, waits for them, and re-layouts  6.99 us (5%)
  Pallas kernels  5.79 us (4%)
    all_to_all x3, blocking collectives, exchanged(): return lax.all_to_all(blocks, axes, split_axis=0, concat_axis=0, tiled=True)  44.2 us
    all_to_all x3, waiting for transfers between devices, exchanged(): return lax.all_to_all(blocks, axes, split_axis=0, concat_axis=0, tiled=True)  26.1 us
    all_to_all x3, starting transfers between devices, exchanged(): return lax.all_to_all(blocks, axes, split_axis=0, concat_axis=0, tiled=True)  20.8 us
    ppermute x9, starting transfers between devices, from_ahead(): lax.ppermute(value, axis, [((i + step) % size, i) for i in range(size)])  15.6 us
    pallas_call x1, Pallas kernels, whole_expert(): pl.pallas_call(expert_body, grid=(units // block,), in_specs=[whole, acro...  5.79 us
    ppermute x4, starting transfers between devices, from_partner(): return lax.ppermute(value, 'tp', [(0, 1), (1, 0)])  5.4 us
    ppermute x9, waiting for transfers between devices, from_ahead(): lax.ppermute(value, axis, [((i + step) % size, i) for i in range(size)])  5.05 us
    add x1, other arithmetic, next_state(): decays[None, :, None, None] * prior_state  4.28 us
  transfers between devices with their start and end apart: 16, of which 6 were waited for; matrix products, arithmetic and copies ran while one was open for 12% of the time, Pallas kernels for 0%

profile of v1, /device:TPU:1, one launch (start us, length us, event | category | flops | bytes accessed | tf_op | source)
XLA Modules:
  0.0 149.2 jit_solution(16111315169851760179)
XLA Ops:
  0.7 1.0 fusion.15
  1.8 0.2 reshape.225
  2.0 0.1 reshape.226
  2.2 2.2 %collective-permute-start.2 = (bf16[16,512]{1,0:T(8,128)(2,1)S(1)}, bf16[16,512]{1,0:T(8,128)(2,1)S(1)}, u32[]{:S(2)}, u32[]{:S(2)}) collective-permute-start(bf16[16,512]{1,0:T(8,128)(2,1)S(1)} %get-tuple-element.63), channel_id=1, source_target_pairs={{24,0},{0,8},{8,16},{16,24},{25,1},{1,9},{9,17},{17,25},{26,2},{2,... | collective-permute-start | bytes 49160 | tf_op jit(solution)/shard_map/ppermute | solution.py:38
  4.4 2.6 %collective-permute-start.1 = (bf16[16,512]{1,0:T(8,128)(2,1)S(1)}, bf16[16,512]{1,0:T(8,128)(2,1)S(1)}, u32[]{:S(2)}, u32[]{:S(2)}) collective-permute-start(bf16[16,512]{1,0:T(8,128)(2,1)S(1)} %get-tuple-element.65), channel_id=1, source_target_pairs={{16,0},{24,8},{0,16},{8,24},{17,1},{25,9},{1,17},{9,25},{18,2},{26... | collective-permute-start | bytes 49160 | tf_op jit(solution)/shard_map/ppermute | solution.py:38
  7.0 1.1 collective-permute-start
  8.1 0.7 bitcast_bitcast_fusion
  8.8 0.8 pad_maximum_fusion
  9.6 0.9 broadcast_in_dim.24
  10.5 11.0 %all-to-all-start = ((bf16[32,16,640]{2,1,0:T(8,128)(2,1)}), bf16[32,16,640]{2,1,0:T(8,128)(2,1)S(1)}, u32[]{:S(2)}, u32[]{:S(2)}) async-start(bf16[32,16,640]{2,1,0:T(8,128)(2,1)} %bitcast.18), calls=%async_computation | async-start | bytes 1310720 | tf_op jit(solution)/shard_map/all_to_all | solution.py:20
  21.8 2.5 %collective-permute-start.3 = (bf16[4,16,512]{2,1,0:T(8,128)(2,1)S(1)}, bf16[4,16,512]{2,1,0:T(8,128)(2,1)S(1)}, u32[]{:S(2)}, u32[]{:S(2)}) collective-permute-start(bf16[4,16,512]{2,1,0:T(8,128)(2,1)S(1)} %get-tuple-element.53), channel_id=1, source_target_pairs={{2,0},{4,2},{6,4},{0,6},{3,1},{5,3},{7,5},{1,7},{10,8},{12,10},{14... | collective-permute-start | bytes 196616 | tf_op jit(solution)/shard_map/ppermute | solution.py:38
  24.3 1.8 %collective-permute-start.4 = (bf16[4,16,512]{2,1,0:T(8,128)(2,1)S(1)}, bf16[4,16,512]{2,1,0:T(8,128)(2,1)S(1)}, u32[]{:S(2)}, u32[]{:S(2)}) collective-permute-start(bf16[4,16,512]{2,1,0:T(8,128)(2,1)S(1)} %get-tuple-element.53), channel_id=1, source_target_pairs={{4,0},{6,2},{0,4},{2,6},{5,1},{7,3},{1,5},{3,7},{12,8},{14,10},{8,... | collective-permute-start | bytes 196616 | tf_op jit(solution)/shard_map/ppermute | solution.py:38
  26.1 4.3 %collective-permute-done.4 = bf16[4,16,512]{2,1,0:T(8,128)(2,1)S(1)} collective-permute-done((bf16[4,16,512]{2,1,0:T(8,128)(2,1)S(1)}, bf16[4,16,512]{2,1,0:T(8,128)(2,1)S(1)}, u32[]{:S(2)}, u32[]{:S(2)}) %collective-permute-start.4) | collective-permute-done | bytes 65568 | tf_op jit(solution)/shard_map/ppermute | solution.py:38
  30.4 0.7 collective-permute-done.5
  31.2 7.9 %all-to-all-done = bf16[32,16,640]{2,1,0:T(8,128)(2,1)S(1)} async-done(((bf16[32,16,640]{2,1,0:T(8,128)(2,1)}), bf16[32,16,640]{2,1,0:T(8,128)(2,1)S(1)}, u32[]{:S(2)}, u32[]{:S(2)}) %all-to-all-start) | async-done | bytes 655392 | tf_op jit(solution)/shard_map/all_to_all | solution.py:20
  39.1 1.7 %collective-permute-start.8 = (bf16[512,128]{1,0:T(8,128)(2,1)S(1)}, bf16[512,128]{1,0:T(8,128)(2,1)S(1)}, u32[]{:S(2)}, u32[]{:S(2)}) collective-permute-start(bf16[512,128]{1,0:T(8,128)(2,1)S(1)} %slice.29), channel_id=1, source_target_pairs={{6,0},{0,2},{2,4},{4,6},{7,1},{1,3},{3,5},{5,7},{14,8},{8,10},{10,... | collective-permute-start | bytes 393224 | tf_op jit(solution)/shard_map/ppermute | solution.py:38
  40.8 1.9 %collective-permute-start.7 = (bf16[512,128]{1,0:T(8,128)(2,1)S(1)}, bf16[512,128]{1,0:T(8,128)(2,1)S(1)}, u32[]{:S(2)}, u32[]{:S(2)}) collective-permute-start(bf16[512,128]{1,0:T(8,128)(2,1)S(1)} %slice.29), channel_id=1, source_target_pairs={{4,0},{6,2},{0,4},{2,6},{5,1},{7,3},{1,5},{3,7},{12,8},{14,10},{8,... | collective-permute-start | bytes 393224 | tf_op jit(solution)/shard_map/ppermute | solution.py:38
  42.6 2.0 %collective-permute-start.6 = (bf16[512,128]{1,0:T(8,128)(2,1)S(1)}, bf16[512,128]{1,0:T(8,128)(2,1)S(1)}, u32[]{:S(2)}, u32[]{:S(2)}) collective-permute-start(bf16[512,128]{1,0:T(8,128)(2,1)S(1)} %slice.29), channel_id=1, source_target_pairs={{2,0},{4,2},{6,4},{0,6},{3,1},{5,3},{7,5},{1,7},{10,8},{12,10},{14... | collective-permute-start | bytes 393224 | tf_op jit(solution)/shard_map/ppermute | solution.py:38
  44.6 1.0 convolution_convert_fusion.2
  45.6 0.1 copy.35
  45.7 0.1 eq.49
  45.8 3.5 %all-to-all-start.1 = ((bf16[16,16,512]{2,1,0:T(8,128)(2,1)}), bf16[16,16,512]{2,1,0:T(8,128)(2,1)S(1)}, u32[]{:S(2)}, u32[]{:S(2)}) async-start(bf16[16,16,512]{2,1,0:T(8,128)(2,1)} %bitcast.20), calls=%async_computation.1 | async-start | bytes 524288 | tf_op jit(solution)/shard_map/all_to_all | solution.py:20
  49.4 0.1 reduce_window_sum.11
  49.5 0.2 select_reduce_fusion.1
  49.7 0.1 eq.55
  49.9 0.1 select_reduce_fusion
  50.0 0.1 fusion.22
  50.2 0.1 multiply_cosine_fusion
  50.3 6.5 %all-to-all-done.1 = bf16[16,16,512]{2,1,0:T(8,128)(2,1)S(1)} async-done(((bf16[16,16,512]{2,1,0:T(8,128)(2,1)}), bf16[16,16,512]{2,1,0:T(8,128)(2,1)S(1)}, u32[]{:S(2)}, u32[]{:S(2)}) %all-to-all-start.1) | async-done | bytes 262176 | tf_op jit(solution)/shard_map/all_to_all | solution.py:20
  57.2 0.1 multiply_subtract_fusion
  57.3 0.1 pad_maximum_fusion.1
  57.5 2.9 %fusion.38 = f32[16,8,1,64]{3,2,1,0:T(1,128)S(1)} fusion(f32[16,8,64,1]{2,3,1,0:T(1,128)S(1)} %bitcast.102, f32[16,8,64,64]{3,2,1,0:T(8,128)} %param.22), kind=kOutput, calls=%fused_computation.112 | convolution fusion | flops 1048576 | bytes 2162688 | tf_op jit(solution)/shard_map/shd,shde->she/dot_general | solution.py:96
  60.4 0.2 multiply_reduce_fusion.1
  60.6 0.1 broadcast_multiply_fusion
  60.9 6.8 %all_to_all.30 = bf16[4,16,512]{2,1,0:T(8,128)(2,1)S(1)} all-to-all(bf16[4,16,512]{2,1,0:T(8,128)(2,1)S(1)} %broadcast_in_dim.28), channel_id=1, replica_groups=mesh['ep_0'=8,'ep_1'=4,'ep_2'=4,'tp'=2] {'ep_1'}, dimensions={0} | all-to-all | bytes 131072 | tf_op jit(solution)/shard_map/all_to_all | solution.py:20
  67.8 0.3 convolution_convert_fusion.3
  68.1 13.4 %all_to_all.31 = bf16[8,16,512]{2,1,0:T(8,128)(2,1)S(1)} all-to-all(bf16[8,16,512]{2,1,0:T(8,128)(2,1)S(1)} %bitcast.105), channel_id=1, replica_groups=mesh['ep_0'=8,'ep_1'=4,'ep_2'=4,'tp'=2] {'ep_1','tp'}, dimensions={0} | all-to-all | bytes 262144 | tf_op jit(solution)/shard_map/all_to_all | solution.py:20
  81.5 0.2 reshape.235
  81.8 0.1 copy.38
  81.9 0.2 reshape.236
  82.1 0.1 fusion.12
  82.2 0.1 fusion.16
  82.3 0.1 fusion.17
  82.5 0.1 fusion.19
  82.5 0.3 convolution_convert_fusion
  82.9 1.0 collective-permute-start.9
  83.8 0.1 collective-permute-start.10
  83.9 0.4 collective-permute-start.11
  84.3 1.2 reshape.237
  85.5 6.2 %all-to-all-start.4 = ((bf16[128,2,1024]{2,1,0:T(2,128)(2,1)}), bf16[128,2,1024]{2,1,0:T(2,128)(2,1)S(1)}, u32[]{:S(2)}, u32[]{:S(2)}) async-start(bf16[128,2,1024]{2,1,0:T(2,128)(2,1)} %reshape.237), calls=%async_computation.4 | async-start | bytes 1048576 | tf_op jit(solution)/shard_map/all_to_all | solution.py:20
  91.7 1.5 fusion.39
  93.2 2.0 %convolution_convert_fusion.1 = bf16[16,2048]{1,0:T(8,128)(2,1)S(1)} fusion(bf16[256,2048]{1,0:T(8,128)(2,1)S(1)} %copy-done, bf16[16,2048]{1,0:T(8,128)(2,1)S(1)} %fusion.19, bf16[2048,256]{1,0:T(8,128)(2,1)} %param.38, f32[16,256]{1,0:T(8,128)S(1)} %fusion.39), kind=kOutput, calls=%fused_computation.3 | convolution fusion | flops 33611776 | bytes 2244608 | tf_op jit(solution)/shard_map/dot_general | solution.py:258
  95.1 4.3 %multiply_add_fusion = f32[16,8,64,64]{3,2,1,0:T(8,128)} fusion(f32[16,8,64,64]{3,2,1,0:T(8,128)} %param.22, f32[16,8,64]{2,1,0:T(8,128)S(1)} %reshape.244, f32[16,8,64]{2,1,0:T(8,128)S(1)} %get-tuple-element.74, f32[8]{0:T(128)S(1)} %dynamic_slice.25), kind=kLoop, calls=%fused_computation.1 | loop fusion | flops 1572864 | bytes 4259872 | tf_op jit(solution)/shard_map/add | solution.py:108
  99.4 11.7 %all-to-all-done.4 = bf16[128,2,1024]{2,1,0:T(2,128)(2,1)S(1)} async-done(((bf16[128,2,1024]{2,1,0:T(2,128)(2,1)}), bf16[128,2,1024]{2,1,0:T(2,128)(2,1)S(1)}, u32[]{:S(2)}, u32[]{:S(2)}) %all-to-all-start.4) | async-done | bytes 524320 | tf_op jit(solution)/shard_map/all_to_all | solution.py:20
  111.1 0.9 copy.42
  112.0 5.8 %shard_map.203 = bf16[128,2048]{1,0:T(8,128)(2,1)} custom-call(bf16[128,2048]{1,0:T(8,128)(2,1)} %bitcast.89, bf16[2048,256]{1,0:T(8,128)(2,1)} %bitcast.93, bf16[2048,256]{1,0:T(8,128)(2,1)} %bitcast.96, bf16[256,2048]{1,0:T(8,128)(2,1)} %bitcast.98, bf16[2048,256]{1,0:T(8,128)(2,1)} %collective-permute-done.9.gate_b, ...), custom_call_target="tpu_custom_call" | custom-call | tf_op jit(solution)/shard_map/pallas_call | solution.py:137
  117.8 1.4 reshape.239
  119.2 23.9 %all_to_all.32 = bf16[128,2,1024]{2,1,0:T(2,128)(2,1)S(1)} all-to-all(bf16[128,2,1024]{2,1,0:T(2,128)(2,1)S(1)} %reshape.239), channel_id=1, replica_groups=mesh['ep_0'=8,'ep_1'=4,'ep_2'=4,'tp'=2] {'ep_0','ep_1','ep_2'}, dimensions={0} | all-to-all | bytes 1048576 | tf_op jit(solution)/shard_map/all_to_all | solution.py:20
  143.1 0.1 copy.43
  143.2 0.2 fusion.40
  143.4 3.9 %collective-permute-start.12 = (f32[16,2048]{1,0:T(8,128)S(1)}, f32[16,2048]{1,0:T(8,128)S(1)}, u32[]{:S(2)}, u32[]{:S(2)}) collective-permute-start(f32[16,2048]{1,0:T(8,128)S(1)} %convert_add_fusion.2), channel_id=1, source_target_pairs={{0,1},{1,0},{2,3},{3,2},{4,5},{5,4},{6,7},{7,6},{8,9},{9,8},{10,11... | collective-permute-start | bytes 393224 | tf_op jit(solution)/shard_map/ppermute | solution.py:28
  147.4 1.0 collective-permute-done.12
  148.3 0.1 multiply_reduce_fusion
  148.5 0.7 fusion.20
  (76 shorter events, 1.2 us)
Async XLA Ops:
  0.6 92.5 %copy-start = (bf16[256,2048]{1,0:T(8,128)(2,1)S(1)}, bf16[256,2048]{1,0:T(8,128)(2,1)}, u32[]{:S(2)}) copy-start(bf16[256,2048]{1,0:T(8,128)(2,1)} %param.39) | copy-start | bytes 3145732
  0.6 49.3 %copy-start.7 = (f32[16,6]{0,1:T(8,128)S(1)}, f32[16,6]{0,1:T(8,128)}, u32[]{:S(2)}) copy-start(f32[16,6]{0,1:T(8,128)} %param.33) | copy-start | bytes 1156
  0.7 44.9 %copy-start.6 = (s32[16,6]{0,1:T(8,128)S(1)}, s32[16,6]{0,1:T(8,128)}, u32[]{:S(2)}) copy-start(s32[16,6]{0,1:T(8,128)} %param.32) | copy-start | bytes 1156
  0.7 49.5 %copy-start.8 = (s32[16]{0:T(128)S(1)}, s32[16]{0:T(128)}, u32[]{:S(2)}) copy-start(s32[16]{0:T(128)} %param.21) | copy-start | bytes 196
  2.2 19.5 %collective-permute-start.2 = (bf16[16,512]{1,0:T(8,128)(2,1)S(1)}, bf16[16,512]{1,0:T(8,128)(2,1)S(1)}, u32[]{:S(2)}, u32[]{:S(2)}) collective-permute-start(bf16[16,512]{1,0:T(8,128)(2,1)S(1)} %get-tuple-element.63), channel_id=1, source_target_pairs={{24,0},{0,8},{8,16},{16,24},{25,1},{1,9},{9,17},{17,25},{26,2},{2,... | collective-permute-start | bytes 49160 | tf_op jit(solution)/shard_map/ppermute | solution.py:38
  4.4 17.3 %collective-permute-start.1 = (bf16[16,512]{1,0:T(8,128)(2,1)S(1)}, bf16[16,512]{1,0:T(8,128)(2,1)S(1)}, u32[]{:S(2)}, u32[]{:S(2)}) collective-permute-start(bf16[16,512]{1,0:T(8,128)(2,1)S(1)} %get-tuple-element.65), channel_id=1, source_target_pairs={{16,0},{24,8},{0,16},{8,24},{17,1},{25,9},{1,17},{9,25},{18,2},{26... | collective-permute-start | bytes 49160 | tf_op jit(solution)/shard_map/ppermute | solution.py:38
  7.0 14.6 %collective-permute-start = (bf16[16,512]{1,0:T(8,128)(2,1)S(1)}, bf16[16,512]{1,0:T(8,128)(2,1)S(1)}, u32[]{:S(2)}, u32[]{:S(2)}) collective-permute-start(bf16[16,512]{1,0:T(8,128)(2,1)S(1)} %get-tuple-element.66), channel_id=1, source_target_pairs={{8,0},{16,8},{24,16},{0,24},{9,1},{17,9},{25,17},{1,25},{10,2},{18... | collective-permute-start | bytes 49160 | tf_op jit(solution)/shard_map/ppermute | solution.py:38
  10.5 28.6 %all-to-all-start = ((bf16[32,16,640]{2,1,0:T(8,128)(2,1)}), bf16[32,16,640]{2,1,0:T(8,128)(2,1)S(1)}, u32[]{:S(2)}, u32[]{:S(2)}) async-start(bf16[32,16,640]{2,1,0:T(8,128)(2,1)} %bitcast.18), calls=%async_computation | async-start | bytes 1310720 | tf_op jit(solution)/shard_map/all_to_all | solution.py:20
  21.8 4.3 %collective-permute-start.3 = (bf16[4,16,512]{2,1,0:T(8,128)(2,1)S(1)}, bf16[4,16,512]{2,1,0:T(8,128)(2,1)S(1)}, u32[]{:S(2)}, u32[]{:S(2)}) collective-permute-start(bf16[4,16,512]{2,1,0:T(8,128)(2,1)S(1)} %get-tuple-element.53), channel_id=1, source_target_pairs={{2,0},{4,2},{6,4},{0,6},{3,1},{5,3},{7,5},{1,7},{10,8},{12,10},{14... | collective-permute-start | bytes 196616 | tf_op jit(solution)/shard_map/ppermute | solution.py:38
  24.3 6.8 %collective-permute-start.5 = (bf16[4,16,512]{2,1,0:T(8,128)(2,1)S(1)}, bf16[4,16,512]{2,1,0:T(8,128)(2,1)S(1)}, u32[]{:S(2)}, u32[]{:S(2)}) collective-permute-start(bf16[4,16,512]{2,1,0:T(8,128)(2,1)S(1)} %get-tuple-element.53), channel_id=1, source_target_pairs={{6,0},{0,2},{2,4},{4,6},{7,1},{1,3},{3,5},{5,7},{14,8},{8,10},{10,... | collective-permute-start | bytes 196616 | tf_op jit(solution)/shard_map/ppermute | solution.py:38
  24.3 6.1 %collective-permute-start.4 = (bf16[4,16,512]{2,1,0:T(8,128)(2,1)S(1)}, bf16[4,16,512]{2,1,0:T(8,128)(2,1)S(1)}, u32[]{:S(2)}, u32[]{:S(2)}) collective-permute-start(bf16[4,16,512]{2,1,0:T(8,128)(2,1)S(1)} %get-tuple-element.53), channel_id=1, source_target_pairs={{4,0},{6,2},{0,4},{2,6},{5,1},{7,3},{1,5},{3,7},{12,8},{14,10},{8,... | collective-permute-start | bytes 196616 | tf_op jit(solution)/shard_map/ppermute | solution.py:38
  39.1 21.8 %collective-permute-start.8 = (bf16[512,128]{1,0:T(8,128)(2,1)S(1)}, bf16[512,128]{1,0:T(8,128)(2,1)S(1)}, u32[]{:S(2)}, u32[]{:S(2)}) collective-permute-start(bf16[512,128]{1,0:T(8,128)(2,1)S(1)} %slice.29), channel_id=1, source_target_pairs={{6,0},{0,2},{2,4},{4,6},{7,1},{1,3},{3,5},{5,7},{14,8},{8,10},{10,... | collective-permute-start | bytes 393224 | tf_op jit(solution)/shard_map/ppermute | solution.py:38
  40.8 20.1 %collective-permute-start.7 = (bf16[512,128]{1,0:T(8,128)(2,1)S(1)}, bf16[512,128]{1,0:T(8,128)(2,1)S(1)}, u32[]{:S(2)}, u32[]{:S(2)}) collective-permute-start(bf16[512,128]{1,0:T(8,128)(2,1)S(1)} %slice.29), channel_id=1, source_target_pairs={{4,0},{6,2},{0,4},{2,6},{5,1},{7,3},{1,5},{3,7},{12,8},{14,10},{8,... | collective-permute-start | bytes 393224 | tf_op jit(solution)/shard_map/ppermute | solution.py:38
  42.6 18.3 %collective-permute-start.6 = (bf16[512,128]{1,0:T(8,128)(2,1)S(1)}, bf16[512,128]{1,0:T(8,128)(2,1)S(1)}, u32[]{:S(2)}, u32[]{:S(2)}) collective-permute-start(bf16[512,128]{1,0:T(8,128)(2,1)S(1)} %slice.29), channel_id=1, source_target_pairs={{2,0},{4,2},{6,4},{0,6},{3,1},{5,3},{7,5},{1,7},{10,8},{12,10},{14... | collective-permute-start | bytes 393224 | tf_op jit(solution)/shard_map/ppermute | solution.py:38
  45.8 11.1 %all-to-all-start.1 = ((bf16[16,16,512]{2,1,0:T(8,128)(2,1)}), bf16[16,16,512]{2,1,0:T(8,128)(2,1)S(1)}, u32[]{:S(2)}, u32[]{:S(2)}) async-start(bf16[16,16,512]{2,1,0:T(8,128)(2,1)} %bitcast.20), calls=%async_computation.1 | async-start | bytes 524288 | tf_op jit(solution)/shard_map/all_to_all | solution.py:20
  57.4 24.8 %copy-start.2 = (bf16[16,2048]{1,0:T(8,128)(2,1)S(1)}, bf16[16,2048]{1,0:T(8,128)(2,1)}, u32[]{:S(2)}) copy-start(bf16[16,2048]{1,0:T(8,128)(2,1)} %param.20) | copy-start | bytes 196612
  57.4 24.8 %copy-start.3 = (f32[2048]{0:T(1024)S(1)}, f32[2048]{0:T(1024)}, u32[]{:S(2)}) copy-start(f32[2048]{0:T(1024)} %param.24) | copy-start | bytes 24580
  57.4 25.0 %copy-start.4 = (f32[2048]{0:T(1024)S(1)}, f32[2048]{0:T(1024)}, u32[]{:S(2)}) copy-start(f32[2048]{0:T(1024)} %param.25) | copy-start | bytes 24580
  57.4 25.4 %copy-start.1 = (bf16[1,2048,256]{2,1,0:T(8,128)(2,1)S(1)}, bf16[1,2048,256]{2,1,0:T(8,128)(2,1)}, u32[]{:S(2)}) copy-start(bf16[1,2048,256]{2,1,0:T(8,128)(2,1)} %param.34) | copy-start | bytes 3145732
  82.9 28.2 %collective-permute-start.9 = (bf16[2048,256]{1,0:T(8,128)(2,1)S(1)}, bf16[2048,256]{1,0:T(8,128)(2,1)}, u32[]{:S(2)}, u32[]{:S(2)}) collective-permute-start(bf16[2048,256]{1,0:T(8,128)(2,1)S(1)} %bitcast.94), channel_id=1, source_target_pairs={{0,1},{1,0},{2,3},{3,2},{4,5},{5,4},{6,7},{7,6},{8,9},{9,8},{10,11... | collective-permute-start | bytes 3145736 | tf_op jit(solution)/shard_map/ppermute | solution.py:28
  83.8 27.2 %collective-permute-start.10 = (bf16[2048,256]{1,0:T(8,128)(2,1)}, bf16[2048,256]{1,0:T(8,128)(2,1)}, u32[]{:S(2)}, u32[]{:S(2)}) collective-permute-start(bf16[2048,256]{1,0:T(8,128)(2,1)} %bitcast.95), channel_id=1, source_target_pairs={{0,1},{1,0},{2,3},{3,2},{4,5},{5,4},{6,7},{7,6},{8,9},{9,8},{10,11... | collective-permute-start | bytes 3145736 | tf_op jit(solution)/shard_map/ppermute | solution.py:28
  83.9 27.1 %collective-permute-start.11 = (bf16[256,2048]{1,0:T(8,128)(2,1)}, bf16[256,2048]{1,0:T(8,128)(2,1)}, u32[]{:S(2)}, u32[]{:S(2)}) collective-permute-start(bf16[256,2048]{1,0:T(8,128)(2,1)} %bitcast.97), channel_id=1, source_target_pairs={{0,1},{1,0},{2,3},{3,2},{4,5},{5,4},{6,7},{7,6},{8,9},{9,8},{10,11... | collective-permute-start | bytes 3145736 | tf_op jit(solution)/shard_map/ppermute | solution.py:28
  85.5 25.6 %all-to-all-start.4 = ((bf16[128,2,1024]{2,1,0:T(2,128)(2,1)}), bf16[128,2,1024]{2,1,0:T(2,128)(2,1)S(1)}, u32[]{:S(2)}, u32[]{:S(2)}) async-start(bf16[128,2,1024]{2,1,0:T(2,128)(2,1)} %reshape.237), calls=%async_computation.4 | async-start | bytes 1048576 | tf_op jit(solution)/shard_map/all_to_all | solution.py:20
  112.0 36.5 %copy-start.5 = (f32[2048]{0:T(1024)S(1)}, f32[2048]{0:T(1024)}, u32[]{:S(2)}) copy-start(f32[2048]{0:T(1024)} %param.26) | copy-start | bytes 24580
  143.4 4.9 %collective-permute-start.12 = (f32[16,2048]{1,0:T(8,128)S(1)}, f32[16,2048]{1,0:T(8,128)S(1)}, u32[]{:S(2)}, u32[]{:S(2)}) collective-permute-start(f32[16,2048]{1,0:T(8,128)S(1)} %convert_add_fusion.2), channel_id=1, source_target_pairs={{0,1},{1,0},{2,3},{3,2},{4,5},{5,4},{6,7},{7,6},{8,9},{9,8},{10,11... | collective-permute-start | bytes 393224 | tf_op jit(solution)/shard_map/ppermute | solution.py:28

commit v2 on v1

--- a/solution.py
+++ b/solution.py
@@ -110,39 +110,43 @@
     )
 
 
-def expert_body(rows, gate_a, up_a, down_a, gate_b, up_b, down_b, out, total):
-    step = pl.program_id(0)
-
-    @pl.when(step == 0)
-    def _():
-        total[...] = jnp.zeros_like(total)
-
-    for gate, up, down in ((gate_a, up_a, down_a), (gate_b, up_b, down_b)):
-        gated = jnp.dot(rows[...], gate[...], preferred_element_type=jnp.float32)
-        lifted = jnp.dot(rows[...], up[...], preferred_element_type=jnp.float32)
-        hidden = (jax.nn.silu(gated) * lifted).astype(jnp.bfloat16)
-        total[...] += jnp.dot(hidden, down[...], preferred_element_type=jnp.float32)
-
-    @pl.when(step == pl.num_programs(0) - 1)
-    def _():
-        out[...] = total[...].astype(jnp.bfloat16)
+def expert_body(rows, *refs):
+    weights, out, held, arrivals = refs[:6], refs[6], refs[7:13], refs[13]
+    copying = [
+        pltpu.make_async_copy(weight, place, arrivals.at[k])
+        for k, (weight, place) in enumerate(zip(weights, held))
+    ]
+    for copy in copying:
+        copy.start()
+
+    def hidden_of(gate_at, up_at):
+        copying[gate_at].wait()
+        gated = jnp.dot(rows[...], held[gate_at][...], preferred_element_type=jnp.float32)
+        copying[up_at].wait()
+        lifted = jnp.dot(rows[...], held[up_at][...], preferred_element_type=jnp.float32)
+        return (jax.nn.silu(gated) * lifted).astype(jnp.bfloat16)
+
+    hidden_here = hidden_of(0, 1)
+    hidden_there = hidden_of(2, 3)
+    copying[4].wait()
+    total = jnp.dot(hidden_here, held[4][...], preferred_element_type=jnp.float32)
+    copying[5].wait()
+    total += jnp.dot(hidden_there, held[5][...], preferred_element_type=jnp.float32)
+    out[...] = total.astype(jnp.bfloat16)
 
 
 def whole_expert(rows, here, there):
-    count, width = rows.shape
-    units, block = here[0].shape[1], 128
-    across = pl.BlockSpec((width, block), lambda i: (0, i))
-    down = pl.BlockSpec((block, width), lambda i: (i, 0))
-    whole = pl.BlockSpec((count, width), lambda i: (0, 0))
+    weights = (*here[:2], *there[:2], here[2], there[2])
     return pl.pallas_call(
         expert_body,
-        grid=(units // block,),
-        in_specs=[whole, across, across, down, across, across, down],
-        out_specs=whole,
-        out_shape=jax.ShapeDtypeStruct((count, width), jnp.bfloat16),
-        scratch_shapes=[pltpu.VMEM((count, width), jnp.float32)],
-        compiler_params=pltpu.CompilerParams(dimension_semantics=("arbitrary",)),
-    )(rows, *here, *there)
+        in_specs=[pl.BlockSpec(memory_space=pltpu.VMEM)]
+        + [pl.BlockSpec(memory_space=pl.ANY)] * len(weights),
+        out_specs=pl.BlockSpec(memory_space=pltpu.VMEM),
+        out_shape=jax.ShapeDtypeStruct(rows.shape, jnp.bfloat16),
+        scratch_shapes=[pltpu.VMEM(weight.shape, weight.dtype) for weight in weights]
+        + [pltpu.SemaphoreType.DMA((len(weights),))],
+        compiler_params=pltpu.CompilerParams(vmem_limit_bytes=52 * 2**20),
+    )(rows, *weights)
 
 
 def on_device(

time: 150 us -> 146 us (0.973)
  Pallas kernels: 5.79 us -> 3.48 us
  local copies, waits for them, and re-layouts: 6.99 us -> 5.15 us
    pallas_call x1, Pallas kernels: 5.79 us -> 3.48 us  [whole_expert(): pl.pallas_call(expert_body, in_specs=[pl.BlockSpec(memory_space=pltpu.VME...]
where the time goes in v2:
time: 146 us; the launch traced here: 145 us
  blocking collectives  44.2 us (30%)
  starting transfers between devices  41.8 us (29%)
  waiting for transfers between devices  32.1 us (22%)
  other arithmetic  8.93 us (6%)
  matrix products  8.14 us (6%)
  local copies, waits for them, and re-layouts  5.15 us (4%)
  Pallas kernels  3.48 us (2%)
    all_to_all x3, blocking collectives, exchanged(): return lax.all_to_all(blocks, axes, split_axis=0, concat_axis=0, tiled=True)  44.2 us
    all_to_all x3, waiting for transfers between devices, exchanged(): return lax.all_to_all(blocks, axes, split_axis=0, concat_axis=0, tiled=True)  26.1 us
    all_to_all x3, starting transfers between devices, exchanged(): return lax.all_to_all(blocks, axes, split_axis=0, concat_axis=0, tiled=True)  20.8 us
    ppermute x9, starting transfers between devices, from_ahead(): lax.ppermute(value, axis, [((i + step) % size, i) for i in range(size)])  15.6 us
    ppermute x4, starting transfers between devices, from_partner(): return lax.ppermute(value, 'tp', [(0, 1), (1, 0)])  5.41 us
    ppermute x9, waiting for transfers between devices, from_ahead(): lax.ppermute(value, axis, [((i + step) % size, i) for i in range(size)])  5.05 us
    add x1, other arithmetic, next_state(): decays[None, :, None, None] * prior_state  4.28 us
    pallas_call x1, Pallas kernels, whole_expert(): pl.pallas_call(expert_body, in_specs=[pl.BlockSpec(memory_space=pltpu.VME...  3.48 us
  transfers between devices with their start and end apart: 16, of which 6 were waited for; matrix products, arithmetic and copies ran while one was open for 12% of the time, Pallas kernels for 0%

profile of v2, /device:TPU:1, one launch (start us, length us, event | category | flops | bytes accessed | tf_op | source)
XLA Modules:
  0.0 145.1 jit_solution(12894675442488449257)
XLA Ops:
  0.7 1.0 fusion.15
  1.8 0.2 reshape.225
  2.0 0.1 reshape.226
  2.2 2.2 %collective-permute-start.2 = (bf16[16,512]{1,0:T(8,128)(2,1)S(1)}, bf16[16,512]{1,0:T(8,128)(2,1)S(1)}, u32[]{:S(2)}, u32[]{:S(2)}) collective-permute-start(bf16[16,512]{1,0:T(8,128)(2,1)S(1)} %get-tuple-element.63), channel_id=1, source_target_pairs={{24,0},{0,8},{8,16},{16,24},{25,1},{1,9},{9,17},{17,25},{26,2},{2,... | collective-permute-start | bytes 49160 | tf_op jit(solution)/shard_map/ppermute | solution.py:38
  4.4 2.6 %collective-permute-start.1 = (bf16[16,512]{1,0:T(8,128)(2,1)S(1)}, bf16[16,512]{1,0:T(8,128)(2,1)S(1)}, u32[]{:S(2)}, u32[]{:S(2)}) collective-permute-start(bf16[16,512]{1,0:T(8,128)(2,1)S(1)} %get-tuple-element.65), channel_id=1, source_target_pairs={{16,0},{24,8},{0,16},{8,24},{17,1},{25,9},{1,17},{9,25},{18,2},{26... | collective-permute-start | bytes 49160 | tf_op jit(solution)/shard_map/ppermute | solution.py:38
  7.0 1.1 collective-permute-start
  8.1 0.7 bitcast_bitcast_fusion
  8.8 0.8 pad_maximum_fusion
  9.6 0.9 broadcast_in_dim.24
  10.5 11.0 %all-to-all-start = ((bf16[32,16,640]{2,1,0:T(8,128)(2,1)}), bf16[32,16,640]{2,1,0:T(8,128)(2,1)S(1)}, u32[]{:S(2)}, u32[]{:S(2)}) async-start(bf16[32,16,640]{2,1,0:T(8,128)(2,1)} %bitcast.18), calls=%async_computation | async-start | bytes 1310720 | tf_op jit(solution)/shard_map/all_to_all | solution.py:20
  21.8 2.5 %collective-permute-start.3 = (bf16[4,16,512]{2,1,0:T(8,128)(2,1)S(1)}, bf16[4,16,512]{2,1,0:T(8,128)(2,1)S(1)}, u32[]{:S(2)}, u32[]{:S(2)}) collective-permute-start(bf16[4,16,512]{2,1,0:T(8,128)(2,1)S(1)} %get-tuple-element.53), channel_id=1, source_target_pairs={{2,0},{4,2},{6,4},{0,6},{3,1},{5,3},{7,5},{1,7},{10,8},{12,10},{14... | collective-permute-start | bytes 196616 | tf_op jit(solution)/shard_map/ppermute | solution.py:38
  24.3 1.8 %collective-permute-start.4 = (bf16[4,16,512]{2,1,0:T(8,128)(2,1)S(1)}, bf16[4,16,512]{2,1,0:T(8,128)(2,1)S(1)}, u32[]{:S(2)}, u32[]{:S(2)}) collective-permute-start(bf16[4,16,512]{2,1,0:T(8,128)(2,1)S(1)} %get-tuple-element.53), channel_id=1, source_target_pairs={{4,0},{6,2},{0,4},{2,6},{5,1},{7,3},{1,5},{3,7},{12,8},{14,10},{8,... | collective-permute-start | bytes 196616 | tf_op jit(solution)/shard_map/ppermute | solution.py:38
  26.1 4.3 %collective-permute-done.4 = bf16[4,16,512]{2,1,0:T(8,128)(2,1)S(1)} collective-permute-done((bf16[4,16,512]{2,1,0:T(8,128)(2,1)S(1)}, bf16[4,16,512]{2,1,0:T(8,128)(2,1)S(1)}, u32[]{:S(2)}, u32[]{:S(2)}) %collective-permute-start.4) | collective-permute-done | bytes 65568 | tf_op jit(solution)/shard_map/ppermute | solution.py:38
  30.4 0.7 collective-permute-done.5
  31.2 7.9 %all-to-all-done = bf16[32,16,640]{2,1,0:T(8,128)(2,1)S(1)} async-done(((bf16[32,16,640]{2,1,0:T(8,128)(2,1)}), bf16[32,16,640]{2,1,0:T(8,128)(2,1)S(1)}, u32[]{:S(2)}, u32[]{:S(2)}) %all-to-all-start) | async-done | bytes 655392 | tf_op jit(solution)/shard_map/all_to_all | solution.py:20
  39.1 1.7 %collective-permute-start.8 = (bf16[512,128]{1,0:T(8,128)(2,1)S(1)}, bf16[512,128]{1,0:T(8,128)(2,1)S(1)}, u32[]{:S(2)}, u32[]{:S(2)}) collective-permute-start(bf16[512,128]{1,0:T(8,128)(2,1)S(1)} %slice.29), channel_id=1, source_target_pairs={{6,0},{0,2},{2,4},{4,6},{7,1},{1,3},{3,5},{5,7},{14,8},{8,10},{10,... | collective-permute-start | bytes 393224 | tf_op jit(solution)/shard_map/ppermute | solution.py:38
  40.8 1.9 %collective-permute-start.7 = (bf16[512,128]{1,0:T(8,128)(2,1)S(1)}, bf16[512,128]{1,0:T(8,128)(2,1)S(1)}, u32[]{:S(2)}, u32[]{:S(2)}) collective-permute-start(bf16[512,128]{1,0:T(8,128)(2,1)S(1)} %slice.29), channel_id=1, source_target_pairs={{4,0},{6,2},{0,4},{2,6},{5,1},{7,3},{1,5},{3,7},{12,8},{14,10},{8,... | collective-permute-start | bytes 393224 | tf_op jit(solution)/shard_map/ppermute | solution.py:38
  42.6 2.0 %collective-permute-start.6 = (bf16[512,128]{1,0:T(8,128)(2,1)S(1)}, bf16[512,128]{1,0:T(8,128)(2,1)S(1)}, u32[]{:S(2)}, u32[]{:S(2)}) collective-permute-start(bf16[512,128]{1,0:T(8,128)(2,1)S(1)} %slice.29), channel_id=1, source_target_pairs={{2,0},{4,2},{6,4},{0,6},{3,1},{5,3},{7,5},{1,7},{10,8},{12,10},{14... | collective-permute-start | bytes 393224 | tf_op jit(solution)/shard_map/ppermute | solution.py:38
  44.6 1.0 convolution_convert_fusion.2
  45.6 0.1 copy.35
  45.7 0.1 eq.49
  45.8 3.5 %all-to-all-start.1 = ((bf16[16,16,512]{2,1,0:T(8,128)(2,1)}), bf16[16,16,512]{2,1,0:T(8,128)(2,1)S(1)}, u32[]{:S(2)}, u32[]{:S(2)}) async-start(bf16[16,16,512]{2,1,0:T(8,128)(2,1)} %bitcast.20), calls=%async_computation.1 | async-start | bytes 524288 | tf_op jit(solution)/shard_map/all_to_all | solution.py:20
  49.4 0.1 reduce_window_sum.11
  49.5 0.2 select_reduce_fusion.1
  49.7 0.1 eq.55
  49.9 0.1 select_reduce_fusion
  50.0 0.1 fusion.22
  50.2 0.1 multiply_cosine_fusion
  50.3 6.5 %all-to-all-done.1 = bf16[16,16,512]{2,1,0:T(8,128)(2,1)S(1)} async-done(((bf16[16,16,512]{2,1,0:T(8,128)(2,1)}), bf16[16,16,512]{2,1,0:T(8,128)(2,1)S(1)}, u32[]{:S(2)}, u32[]{:S(2)}) %all-to-all-start.1) | async-done | bytes 262176 | tf_op jit(solution)/shard_map/all_to_all | solution.py:20
  57.2 0.1 multiply_subtract_fusion
  57.3 0.1 pad_maximum_fusion.1
  57.5 2.9 %fusion.38 = f32[16,8,1,64]{3,2,1,0:T(1,128)S(1)} fusion(f32[16,8,64,1]{2,3,1,0:T(1,128)S(1)} %bitcast.102, f32[16,8,64,64]{3,2,1,0:T(8,128)} %param.22), kind=kOutput, calls=%fused_computation.112 | convolution fusion | flops 1048576 | bytes 2162688 | tf_op jit(solution)/shard_map/shd,shde->she/dot_general | solution.py:96
  60.4 0.2 multiply_reduce_fusion.1
  60.6 0.1 broadcast_multiply_fusion
  60.9 6.8 %all_to_all.30 = bf16[4,16,512]{2,1,0:T(8,128)(2,1)S(1)} all-to-all(bf16[4,16,512]{2,1,0:T(8,128)(2,1)S(1)} %broadcast_in_dim.28), channel_id=1, replica_groups=mesh['ep_0'=8,'ep_1'=4,'ep_2'=4,'tp'=2] {'ep_1'}, dimensions={0} | all-to-all | bytes 131072 | tf_op jit(solution)/shard_map/all_to_all | solution.py:20
  67.8 0.3 convolution_convert_fusion.3
  68.1 13.4 %all_to_all.31 = bf16[8,16,512]{2,1,0:T(8,128)(2,1)S(1)} all-to-all(bf16[8,16,512]{2,1,0:T(8,128)(2,1)S(1)} %bitcast.105), channel_id=1, replica_groups=mesh['ep_0'=8,'ep_1'=4,'ep_2'=4,'tp'=2] {'ep_1','tp'}, dimensions={0} | all-to-all | bytes 262144 | tf_op jit(solution)/shard_map/all_to_all | solution.py:20
  81.5 0.2 reshape.235
  81.8 0.1 copy.38
  81.9 0.2 reshape.236
  82.1 0.1 fusion.12
  82.2 0.1 fusion.16
  82.3 0.1 fusion.17
  82.5 0.1 fusion.19
  82.5 0.3 convolution_convert_fusion
  82.9 1.0 collective-permute-start.9
  83.8 0.1 collective-permute-start.10
  83.9 0.4 collective-permute-start.11
  84.3 1.2 reshape.237
  85.5 6.2 %all-to-all-start.4 = ((bf16[128,2,1024]{2,1,0:T(2,128)(2,1)}), bf16[128,2,1024]{2,1,0:T(2,128)(2,1)S(1)}, u32[]{:S(2)}, u32[]{:S(2)}) async-start(bf16[128,2,1024]{2,1,0:T(2,128)(2,1)} %reshape.237), calls=%async_computation.4 | async-start | bytes 1048576 | tf_op jit(solution)/shard_map/all_to_all | solution.py:20
  91.7 1.5 %fusion.39 = f32[16,256]{1,0:T(8,128)S(1)} fusion(bf16[16,2048]{1,0:T(8,128)(2,1)S(1)} %fusion.19, bf16[2048,256]{1,0:T(8,128)(2,1)} %param.37), kind=kOutput, calls=%fused_computation.113 | convolution fusion | flops 16777216 | bytes 1130496 | tf_op jit(solution)/shard_map/dot_general | solution.py:259
  93.2 2.0 %convolution_convert_fusion.1 = bf16[16,2048]{1,0:T(8,128)(2,1)S(1)} fusion(bf16[256,2048]{1,0:T(8,128)(2,1)S(1)} %copy-done, bf16[16,2048]{1,0:T(8,128)(2,1)S(1)} %fusion.19, bf16[2048,256]{1,0:T(8,128)(2,1)} %param.38, f32[16,256]{1,0:T(8,128)S(1)} %fusion.39), kind=kOutput, calls=%fused_computation.3 | convolution fusion | flops 33611776 | bytes 2244608 | tf_op jit(solution)/shard_map/dot_general | solution.py:262
  95.1 4.3 %multiply_add_fusion = f32[16,8,64,64]{3,2,1,0:T(8,128)} fusion(f32[16,8,64,64]{3,2,1,0:T(8,128)} %param.22, f32[16,8,64]{2,1,0:T(8,128)S(1)} %reshape.244, f32[16,8,64]{2,1,0:T(8,128)S(1)} %get-tuple-element.74, f32[8]{0:T(128)S(1)} %dynamic_slice.25), kind=kLoop, calls=%fused_computation.1 | loop fusion | flops 1572864 | bytes 4259872 | tf_op jit(solution)/shard_map/add | solution.py:108
  99.4 11.7 %all-to-all-done.4 = bf16[128,2,1024]{2,1,0:T(2,128)(2,1)S(1)} async-done(((bf16[128,2,1024]{2,1,0:T(2,128)(2,1)}), bf16[128,2,1024]{2,1,0:T(2,128)(2,1)S(1)}, u32[]{:S(2)}, u32[]{:S(2)}) %all-to-all-start.4) | async-done | bytes 524320 | tf_op jit(solution)/shard_map/all_to_all | solution.py:20
  111.1 0.1 copy.42
  111.2 3.5 %shard_map.203 = bf16[128,2048]{1,0:T(8,128)(2,1)S(1)} custom-call(bf16[128,2048]{1,0:T(8,128)(2,1)S(1)} %bitcast.89, bf16[2048,256]{1,0:T(8,128)(2,1)} %bitcast.93, bf16[2048,256]{1,0:T(8,128)(2,1)} %bitcast.96, bf16[2048,256]{1,0:T(8,128)(2,1)} %collective-permute-done.9.refs_2_, bf16[2048,256]{1,0:T(8,128)(2,1)} %collective-permute-done.10.refs_3_, ...), custom_call_target="tpu_custom_call" | custom-call | tf_op jit(solution)/shard_map/pallas_call | solution.py:140
  114.7 0.4 reshape.239
  115.1 23.9 %all_to_all.32 = bf16[128,2,1024]{2,1,0:T(2,128)(2,1)S(1)} all-to-all(bf16[128,2,1024]{2,1,0:T(2,128)(2,1)S(1)} %reshape.239), channel_id=1, replica_groups=mesh['ep_0'=8,'ep_1'=4,'ep_2'=4,'tp'=2] {'ep_0','ep_1','ep_2'}, dimensions={0} | all-to-all | bytes 1048576 | tf_op jit(solution)/shard_map/all_to_all | solution.py:20
  138.9 0.1 copy.43
  139.1 0.2 fusion.40
  139.3 3.9 %collective-permute-start.12 = (f32[16,2048]{1,0:T(8,128)S(1)}, f32[16,2048]{1,0:T(8,128)S(1)}, u32[]{:S(2)}, u32[]{:S(2)}) collective-permute-start(f32[16,2048]{1,0:T(8,128)S(1)} %convert_add_fusion.2), channel_id=1, source_target_pairs={{0,1},{1,0},{2,3},{3,2},{4,5},{5,4},{6,7},{7,6},{8,9},{9,8},{10,11... | collective-permute-start | bytes 393224 | tf_op jit(solution)/shard_map/ppermute | solution.py:28
  143.2 1.0 collective-permute-done.12
  144.2 0.1 multiply_reduce_fusion
  144.4 0.7 fusion.20
  (76 shorter events, 1.2 us)
Async XLA Ops:
  0.6 92.5 %copy-start = (bf16[256,2048]{1,0:T(8,128)(2,1)S(1)}, bf16[256,2048]{1,0:T(8,128)(2,1)}, u32[]{:S(2)}) copy-start(bf16[256,2048]{1,0:T(8,128)(2,1)} %param.39) | copy-start | bytes 3145732
  0.6 49.3 %copy-start.7 = (f32[16,6]{0,1:T(8,128)S(1)}, f32[16,6]{0,1:T(8,128)}, u32[]{:S(2)}) copy-start(f32[16,6]{0,1:T(8,128)} %param.33) | copy-start | bytes 1156
  0.7 44.9 %copy-start.6 = (s32[16,6]{0,1:T(8,128)S(1)}, s32[16,6]{0,1:T(8,128)}, u32[]{:S(2)}) copy-start(s32[16,6]{0,1:T(8,128)} %param.32) | copy-start | bytes 1156
  0.7 49.5 %copy-start.8 = (s32[16]{0:T(128)S(1)}, s32[16]{0:T(128)}, u32[]{:S(2)}) copy-start(s32[16]{0:T(128)} %param.21) | copy-start | bytes 196
  2.2 19.5 %collective-permute-start.2 = (bf16[16,512]{1,0:T(8,128)(2,1)S(1)}, bf16[16,512]{1,0:T(8,128)(2,1)S(1)}, u32[]{:S(2)}, u32[]{:S(2)}) collective-permute-start(bf16[16,512]{1,0:T(8,128)(2,1)S(1)} %get-tuple-element.63), channel_id=1, source_target_pairs={{24,0},{0,8},{8,16},{16,24},{25,1},{1,9},{9,17},{17,25},{26,2},{2,... | collective-permute-start | bytes 49160 | tf_op jit(solution)/shard_map/ppermute | solution.py:38
  4.4 17.3 %collective-permute-start.1 = (bf16[16,512]{1,0:T(8,128)(2,1)S(1)}, bf16[16,512]{1,0:T(8,128)(2,1)S(1)}, u32[]{:S(2)}, u32[]{:S(2)}) collective-permute-start(bf16[16,512]{1,0:T(8,128)(2,1)S(1)} %get-tuple-element.65), channel_id=1, source_target_pairs={{16,0},{24,8},{0,16},{8,24},{17,1},{25,9},{1,17},{9,25},{18,2},{26... | collective-permute-start | bytes 49160 | tf_op jit(solution)/shard_map/ppermute | solution.py:38
  7.0 14.6 %collective-permute-start = (bf16[16,512]{1,0:T(8,128)(2,1)S(1)}, bf16[16,512]{1,0:T(8,128)(2,1)S(1)}, u32[]{:S(2)}, u32[]{:S(2)}) collective-permute-start(bf16[16,512]{1,0:T(8,128)(2,1)S(1)} %get-tuple-element.66), channel_id=1, source_target_pairs={{8,0},{16,8},{24,16},{0,24},{9,1},{17,9},{25,17},{1,25},{10,2},{18... | collective-permute-start | bytes 49160 | tf_op jit(solution)/shard_map/ppermute | solution.py:38
  10.5 28.6 %all-to-all-start = ((bf16[32,16,640]{2,1,0:T(8,128)(2,1)}), bf16[32,16,640]{2,1,0:T(8,128)(2,1)S(1)}, u32[]{:S(2)}, u32[]{:S(2)}) async-start(bf16[32,16,640]{2,1,0:T(8,128)(2,1)} %bitcast.18), calls=%async_computation | async-start | bytes 1310720 | tf_op jit(solution)/shard_map/all_to_all | solution.py:20
  21.8 4.3 %collective-permute-start.3 = (bf16[4,16,512]{2,1,0:T(8,128)(2,1)S(1)}, bf16[4,16,512]{2,1,0:T(8,128)(2,1)S(1)}, u32[]{:S(2)}, u32[]{:S(2)}) collective-permute-start(bf16[4,16,512]{2,1,0:T(8,128)(2,1)S(1)} %get-tuple-element.53), channel_id=1, source_target_pairs={{2,0},{4,2},{6,4},{0,6},{3,1},{5,3},{7,5},{1,7},{10,8},{12,10},{14... | collective-permute-start | bytes 196616 | tf_op jit(solution)/shard_map/ppermute | solution.py:38
  24.3 6.8 %collective-permute-start.5 = (bf16[4,16,512]{2,1,0:T(8,128)(2,1)S(1)}, bf16[4,16,512]{2,1,0:T(8,128)(2,1)S(1)}, u32[]{:S(2)}, u32[]{:S(2)}) collective-permute-start(bf16[4,16,512]{2,1,0:T(8,128)(2,1)S(1)} %get-tuple-element.53), channel_id=1, source_target_pairs={{6,0},{0,2},{2,4},{4,6},{7,1},{1,3},{3,5},{5,7},{14,8},{8,10},{10,... | collective-permute-start | bytes 196616 | tf_op jit(solution)/shard_map/ppermute | solution.py:38
  24.3 6.1 %collective-permute-start.4 = (bf16[4,16,512]{2,1,0:T(8,128)(2,1)S(1)}, bf16[4,16,512]{2,1,0:T(8,128)(2,1)S(1)}, u32[]{:S(2)}, u32[]{:S(2)}) collective-permute-start(bf16[4,16,512]{2,1,0:T(8,128)(2,1)S(1)} %get-tuple-element.53), channel_id=1, source_target_pairs={{4,0},{6,2},{0,4},{2,6},{5,1},{7,3},{1,5},{3,7},{12,8},{14,10},{8,... | collective-permute-start | bytes 196616 | tf_op jit(solution)/shard_map/ppermute | solution.py:38
  39.1 21.8 %collective-permute-start.8 = (bf16[512,128]{1,0:T(8,128)(2,1)S(1)}, bf16[512,128]{1,0:T(8,128)(2,1)S(1)}, u32[]{:S(2)}, u32[]{:S(2)}) collective-permute-start(bf16[512,128]{1,0:T(8,128)(2,1)S(1)} %slice.29), channel_id=1, source_target_pairs={{6,0},{0,2},{2,4},{4,6},{7,1},{1,3},{3,5},{5,7},{14,8},{8,10},{10,... | collective-permute-start | bytes 393224 | tf_op jit(solution)/shard_map/ppermute | solution.py:38
  40.8 20.1 %collective-permute-start.7 = (bf16[512,128]{1,0:T(8,128)(2,1)S(1)}, bf16[512,128]{1,0:T(8,128)(2,1)S(1)}, u32[]{:S(2)}, u32[]{:S(2)}) collective-permute-start(bf16[512,128]{1,0:T(8,128)(2,1)S(1)} %slice.29), channel_id=1, source_target_pairs={{4,0},{6,2},{0,4},{2,6},{5,1},{7,3},{1,5},{3,7},{12,8},{14,10},{8,... | collective-permute-start | bytes 393224 | tf_op jit(solution)/shard_map/ppermute | solution.py:38
  42.6 18.3 %collective-permute-start.6 = (bf16[512,128]{1,0:T(8,128)(2,1)S(1)}, bf16[512,128]{1,0:T(8,128)(2,1)S(1)}, u32[]{:S(2)}, u32[]{:S(2)}) collective-permute-start(bf16[512,128]{1,0:T(8,128)(2,1)S(1)} %slice.29), channel_id=1, source_target_pairs={{2,0},{4,2},{6,4},{0,6},{3,1},{5,3},{7,5},{1,7},{10,8},{12,10},{14... | collective-permute-start | bytes 393224 | tf_op jit(solution)/shard_map/ppermute | solution.py:38
  45.8 11.1 %all-to-all-start.1 = ((bf16[16,16,512]{2,1,0:T(8,128)(2,1)}), bf16[16,16,512]{2,1,0:T(8,128)(2,1)S(1)}, u32[]{:S(2)}, u32[]{:S(2)}) async-start(bf16[16,16,512]{2,1,0:T(8,128)(2,1)} %bitcast.20), calls=%async_computation.1 | async-start | bytes 524288 | tf_op jit(solution)/shard_map/all_to_all | solution.py:20
  57.4 24.8 %copy-start.2 = (bf16[16,2048]{1,0:T(8,128)(2,1)S(1)}, bf16[16,2048]{1,0:T(8,128)(2,1)}, u32[]{:S(2)}) copy-start(bf16[16,2048]{1,0:T(8,128)(2,1)} %param.20) | copy-start | bytes 196612
  57.4 24.8 %copy-start.3 = (f32[2048]{0:T(1024)S(1)}, f32[2048]{0:T(1024)}, u32[]{:S(2)}) copy-start(f32[2048]{0:T(1024)} %param.24) | copy-start | bytes 24580
  57.4 25.0 %copy-start.4 = (f32[2048]{0:T(1024)S(1)}, f32[2048]{0:T(1024)}, u32[]{:S(2)}) copy-start(f32[2048]{0:T(1024)} %param.25) | copy-start | bytes 24580
  57.4 25.4 %copy-start.1 = (bf16[1,2048,256]{2,1,0:T(8,128)(2,1)S(1)}, bf16[1,2048,256]{2,1,0:T(8,128)(2,1)}, u32[]{:S(2)}) copy-start(bf16[1,2048,256]{2,1,0:T(8,128)(2,1)} %param.34) | copy-start | bytes 3145732
  82.9 28.2 %collective-permute-start.9 = (bf16[2048,256]{1,0:T(8,128)(2,1)S(1)}, bf16[2048,256]{1,0:T(8,128)(2,1)}, u32[]{:S(2)}, u32[]{:S(2)}) collective-permute-start(bf16[2048,256]{1,0:T(8,128)(2,1)S(1)} %bitcast.94), channel_id=1, source_target_pairs={{0,1},{1,0},{2,3},{3,2},{4,5},{5,4},{6,7},{7,6},{8,9},{9,8},{10,11... | collective-permute-start | bytes 3145736 | tf_op jit(solution)/shard_map/ppermute | solution.py:28
  83.8 27.2 %collective-permute-start.10 = (bf16[2048,256]{1,0:T(8,128)(2,1)}, bf16[2048,256]{1,0:T(8,128)(2,1)}, u32[]{:S(2)}, u32[]{:S(2)}) collective-permute-start(bf16[2048,256]{1,0:T(8,128)(2,1)} %bitcast.95), channel_id=1, source_target_pairs={{0,1},{1,0},{2,3},{3,2},{4,5},{5,4},{6,7},{7,6},{8,9},{9,8},{10,11... | collective-permute-start | bytes 3145736 | tf_op jit(solution)/shard_map/ppermute | solution.py:28
  83.9 27.1 %collective-permute-start.11 = (bf16[256,2048]{1,0:T(8,128)(2,1)}, bf16[256,2048]{1,0:T(8,128)(2,1)}, u32[]{:S(2)}, u32[]{:S(2)}) collective-permute-start(bf16[256,2048]{1,0:T(8,128)(2,1)} %bitcast.97), channel_id=1, source_target_pairs={{0,1},{1,0},{2,3},{3,2},{4,5},{5,4},{6,7},{7,6},{8,9},{9,8},{10,11... | collective-permute-start | bytes 3145736 | tf_op jit(solution)/shard_map/ppermute | solution.py:28
  85.5 25.6 %all-to-all-start.4 = ((bf16[128,2,1024]{2,1,0:T(2,128)(2,1)}), bf16[128,2,1024]{2,1,0:T(2,128)(2,1)S(1)}, u32[]{:S(2)}, u32[]{:S(2)}) async-start(bf16[128,2,1024]{2,1,0:T(2,128)(2,1)} %reshape.237), calls=%async_computation.4 | async-start | bytes 1048576 | tf_op jit(solution)/shard_map/all_to_all | solution.py:20
  111.2 33.2 %copy-start.5 = (f32[2048]{0:T(1024)S(1)}, f32[2048]{0:T(1024)}, u32[]{:S(2)}) copy-start(f32[2048]{0:T(1024)} %param.26) | copy-start | bytes 24580
  139.3 4.9 %collective-permute-start.12 = (f32[16,2048]{1,0:T(8,128)S(1)}, f32[16,2048]{1,0:T(8,128)S(1)}, u32[]{:S(2)}, u32[]{:S(2)}) collective-permute-start(f32[16,2048]{1,0:T(8,128)S(1)} %convert_add_fusion.2), channel_id=1, source_target_pairs={{0,1},{1,0},{2,3},{3,2},{4,5},{5,4},{6,7},{7,6},{8,9},{9,8},{10,11... | collective-permute-start | bytes 393224 | tf_op jit(solution)/shard_map/ppermute | solution.py:28

commit v3 on v2

--- a/solution.py
+++ b/solution.py
@@ -147,6 +147,30 @@
         + [pltpu.SemaphoreType.DMA((len(weights),))],
         compiler_params=pltpu.CompilerParams(vmem_limit_bytes=52 * 2**20),
     )(rows, *weights)
+
+
+def pack_body(query, key, value, gate, wout, tokens, gain, sent, gained):
+    turned = wout[...].astype(jnp.float32).T.astype(jnp.bfloat16)
+    cols = query.shape[1]
+    share = sent.shape[2] - cols
+    kinds = (query, key, value, gate)
+    for place in range(sent.shape[0]):
+        k = place % len(kinds)
+        sent[place, :, :cols] = kinds[k][...]
+        sent[place, :, cols:] = turned[:, k * share : (k + 1) * share]
+    gained[...] = (tokens[...].astype(jnp.float32) * gain[...]).astype(jnp.bfloat16)
+
+
+def packed(kinds, out_weight, tokens, gain, depth):
+    rows, cols = kinds[0].shape
+    count = len(kinds)
+    return pl.pallas_call(
+        pack_body,
+        out_shape=(
+            jax.ShapeDtypeStruct((depth * count, rows, cols + cols // count), jnp.bfloat16),
+            jax.ShapeDtypeStruct(tokens.shape, jnp.bfloat16),
+        ),
+    )(*kinds, out_weight, tokens, gain[None, :])
 
 
 def on_device(
@@ -178,18 +202,16 @@
     plane = rows_y * rows_x
     core = lax.axis_index("tp")
 
-    kinds = jnp.stack([query_weight, key_weight, value_weight, gate_weight])
     share = cols // rows_x
-    wout_parts = out_weight.reshape(rows_x, share, -1).swapaxes(1, 2)
-    sent = copies(jnp.concatenate([kinds, wout_parts], axis=2), depth)
-    held = exchanged(sent.reshape(depth * rows_x, -1, cols + share), (Z, X))
+    kinds = (query_weight, key_weight, value_weight, gate_weight)
+    sent, gained = packed(kinds, out_weight, tokens, mix_gain, depth)
+    held = exchanged(sent, (Z, X))
     held = held.reshape(-1, cols + share)
     kind_weight = held[:, :cols]
     wout_part = held[:, cols:]
     others = [from_ahead(wout_part, X, step) for step in range(1, rows_x)]
 
     wide_tokens = tokens.astype(jnp.float32)
-    gained = (wide_tokens * mix_gain).astype(jnp.bfloat16)
     by_y = gained.reshape(seq_here, depth, rows_y, -1).transpose(2, 0, 1, 3)
     plane_rows = plane_tokens(by_y.reshape(rows_y, seq_here, width // rows_y))
     projected = jnp.dot(

time: 146 us -> 143 us (0.979)
  waiting for transfers between devices: 32.1 us -> 25.8 us
  Pallas kernels: 3.48 us -> 5.44 us
  starting transfers between devices: 41.8 us -> 43.7 us
    all_to_all x3, waiting for transfers between devices: 26.1 us -> 20.1 us  [exchanged(): return lax.all_to_all(blocks, axes, split_axis=0, concat_axis=0, tiled=True)]
    all_to_all x3, starting transfers between devices: 20.8 us -> 24.5 us  [exchanged(): return lax.all_to_all(blocks, axes, split_axis=0, concat_axis=0, tiled=True)]
    pallas_call x0 -> x1, Pallas kernels: none -> 1.96 us  [packed(): pl.pallas_call(pack_body, out_shape=(jax.ShapeDtypeStruct((depth * count,...]
    ppermute x9, starting transfers between devices: 15.6 us -> 13.8 us  [from_ahead(): lax.ppermute(value, axis, [((i + step) % size, i) for i in range(size)])]
    unnamed x33 -> x34, local copies, waits for them, and re-layouts: 0.36 us -> 1.91 us
  transfers between devices with their start and end apart: 16 -> 16, of which waited for: 6 -> 7; matrix products, arithmetic and copies ran while one was open for 12% -> 12% of each run, Pallas kernels for 0% -> 0%
where the time goes in v3:
time: 143 us
  blocking collectives  44.5 us (31%)
  starting transfers between devices  43.7 us (31%)
  waiting for transfers between devices  25.8 us (18%)
  matrix products  8.14 us (6%)
  other arithmetic  8.07 us (6%)
  local copies, waits for them, and re-layouts  5.93 us (4%)
  Pallas kernels  5.44 us (4%)
    all_to_all x3, blocking collectives, exchanged(): return lax.all_to_all(blocks, axes, split_axis=0, concat_axis=0, tiled=True)  44.5 us
    all_to_all x3, starting transfers between devices, exchanged(): return lax.all_to_all(blocks, axes, split_axis=0, concat_axis=0, tiled=True)  24.5 us
    all_to_all x3, waiting for transfers between devices, exchanged(): return lax.all_to_all(blocks, axes, split_axis=0, concat_axis=0, tiled=True)  20.1 us
    ppermute x9, starting transfers between devices, from_ahead(): lax.ppermute(value, axis, [((i + step) % size, i) for i in range(size)])  13.8 us
    ppermute x4, starting transfers between devices, from_partner(): return lax.ppermute(value, 'tp', [(0, 1), (1, 0)])  5.42 us
    ppermute x9, waiting for transfers between devices, from_ahead(): lax.ppermute(value, axis, [((i + step) % size, i) for i in range(size)])  4.69 us
    add x1, other arithmetic, next_state(): decays[None, :, None, None] * prior_state  4.28 us
    pallas_call x1, Pallas kernels, whole_expert(): pl.pallas_call(expert_body, in_specs=[pl.BlockSpec(memory_space=pltpu.VME...  3.48 us
  transfers between devices with their start and end apart: 16, of which 7 were waited for; matrix products, arithmetic and copies ran while one was open for 12% of the time, Pallas kernels for 0%

profile of v3, /device:TPU:1, one launch (start us, length us, event | category | flops | bytes accessed | tf_op | source)
XLA Modules:
  0.0 142.8 jit_solution(12601768045350332278)
XLA Ops:
  0.7 1.5 %copy.32.wout = bf16[512,16]{1,0:T(8,128)(2,1)} copy(bf16[512,16]{0,1:T(8,128)(2,1)} %param.31) | data formatting | bytes 32768 | tf_op args[11]
  2.2 2.0 %shard_map.203 = (bf16[32,16,640]{2,1,0:T(8,128)(2,1)}, bf16[16,2048]{1,0:T(8,128)(2,1)}) custom-call(bf16[16,512]{1,0:T(8,128)(2,1)} %query.1, bf16[16,512]{1,0:T(8,128)(2,1)} %key.1, bf16[16,512]{1,0:T(8,128)(2,1)} %value.1, bf16[16,512]{1,0:T(8,128)(2,1)} %gate.1, bf16[512,16]{1,0:T(8,128)(2,1)} %copy.32.wout, bf16[16,2048]{1,0:T(8,128)(2,1)} %tokens.1, ...), custom_call_target="tpu_custom_call" | custom-call | tf_op jit(solution)/shard_map/pallas_call | solution.py:167
  4.2 11.9 %all-to-all-start = ((bf16[32,16,640]{2,1,0:T(8,128)(2,1)}), bf16[32,16,640]{2,1,0:T(8,128)(2,1)S(1)}, u32[]{:S(2)}, u32[]{:S(2)}) async-start(bf16[32,16,640]{2,1,0:T(8,128)(2,1)} %get-tuple-element.29), calls=%async_computation | async-start | bytes 1310720 | tf_op jit(solution)/shard_map/all_to_all | solution.py:20
  16.1 1.0 reshape.218
  17.2 0.1 reshape.219
  17.4 1.4 collective-permute-start.2
  18.7 2.6 %collective-permute-start.1 = (bf16[16,512]{1,0:T(8,128)(2,1)S(1)}, bf16[16,512]{1,0:T(8,128)(2,1)S(1)}, u32[]{:S(2)}, u32[]{:S(2)}) collective-permute-start(bf16[16,512]{1,0:T(8,128)(2,1)S(1)} %get-tuple-element.67), channel_id=1, source_target_pairs={{16,0},{24,8},{0,16},{8,24},{17,1},{25,9},{1,17},{9,25},{18,2},{26... | collective-permute-start | bytes 49160 | tf_op jit(solution)/shard_map/ppermute | solution.py:38
  21.4 1.1 collective-permute-start
  22.4 1.0 fusion.12
  23.5 0.7 collective-permute-done
  24.3 2.5 %collective-permute-start.3 = (bf16[4,16,512]{2,1,0:T(8,128)(2,1)S(1)}, bf16[4,16,512]{2,1,0:T(8,128)(2,1)S(1)}, u32[]{:S(2)}, u32[]{:S(2)}) collective-permute-start(bf16[4,16,512]{2,1,0:T(8,128)(2,1)S(1)} %get-tuple-element.57), channel_id=1, source_target_pairs={{2,0},{4,2},{6,4},{0,6},{3,1},{5,3},{7,5},{1,7},{10,8},{12,10},{14... | collective-permute-start | bytes 196616 | tf_op jit(solution)/shard_map/ppermute | solution.py:38
  26.9 1.8 %collective-permute-start.4 = (bf16[4,16,512]{2,1,0:T(8,128)(2,1)S(1)}, bf16[4,16,512]{2,1,0:T(8,128)(2,1)S(1)}, u32[]{:S(2)}, u32[]{:S(2)}) collective-permute-start(bf16[4,16,512]{2,1,0:T(8,128)(2,1)S(1)} %get-tuple-element.57), channel_id=1, source_target_pairs={{4,0},{6,2},{0,4},{2,6},{5,1},{7,3},{1,5},{3,7},{12,8},{14,10},{8,... | collective-permute-start | bytes 196616 | tf_op jit(solution)/shard_map/ppermute | solution.py:38
  28.7 3.8 %collective-permute-done.4 = bf16[4,16,512]{2,1,0:T(8,128)(2,1)S(1)} collective-permute-done((bf16[4,16,512]{2,1,0:T(8,128)(2,1)S(1)}, bf16[4,16,512]{2,1,0:T(8,128)(2,1)S(1)}, u32[]{:S(2)}, u32[]{:S(2)}) %collective-permute-start.4) | collective-permute-done | bytes 65568 | tf_op jit(solution)/shard_map/ppermute | solution.py:38
  32.5 0.2 collective-permute-done.5
  32.8 2.1 %all-to-all-done = bf16[32,16,640]{2,1,0:T(8,128)(2,1)S(1)} async-done(((bf16[32,16,640]{2,1,0:T(8,128)(2,1)}), bf16[32,16,640]{2,1,0:T(8,128)(2,1)S(1)}, u32[]{:S(2)}, u32[]{:S(2)}) %all-to-all-start) | async-done | bytes 655392 | tf_op jit(solution)/shard_map/all_to_all | solution.py:20
  34.9 0.9 collective-permute-start.8
  35.8 2.6 %collective-permute-start.7 = (bf16[512,128]{1,0:T(8,128)(2,1)S(1)}, bf16[512,128]{1,0:T(8,128)(2,1)S(1)}, u32[]{:S(2)}, u32[]{:S(2)}) collective-permute-start(bf16[512,128]{1,0:T(8,128)(2,1)S(1)} %slice.29), channel_id=1, source_target_pairs={{4,0},{6,2},{0,4},{2,6},{5,1},{7,3},{1,5},{3,7},{12,8},{14,10},{8,... | collective-permute-start | bytes 393224 | tf_op jit(solution)/shard_map/ppermute | solution.py:38
  38.4 1.0 collective-permute-start.6
  39.4 1.0 convolution_convert_fusion.2
  40.4 0.1 copy.35
  40.5 0.1 eq.49
  40.5 4.5 %all-to-all-start.1 = ((bf16[16,16,512]{2,1,0:T(8,128)(2,1)}), bf16[16,16,512]{2,1,0:T(8,128)(2,1)S(1)}, u32[]{:S(2)}, u32[]{:S(2)}) async-start(bf16[16,16,512]{2,1,0:T(8,128)(2,1)} %bitcast.15), calls=%async_computation.1 | async-start | bytes 524288 | tf_op jit(solution)/shard_map/all_to_all | solution.py:20
  45.2 0.1 reduce_window_sum.11
  45.3 0.2 select_reduce_fusion.1
  45.5 0.1 eq.55
  45.7 0.1 select_reduce_fusion
  45.8 0.1 fusion.21
  45.9 0.1 multiply_cosine_fusion
  46.0 6.6 %all-to-all-done.1 = bf16[16,16,512]{2,1,0:T(8,128)(2,1)S(1)} async-done(((bf16[16,16,512]{2,1,0:T(8,128)(2,1)}), bf16[16,16,512]{2,1,0:T(8,128)(2,1)S(1)}, u32[]{:S(2)}, u32[]{:S(2)}) %all-to-all-start.1) | async-done | bytes 262176 | tf_op jit(solution)/shard_map/all_to_all | solution.py:20
  53.0 0.1 multiply_subtract_fusion
  53.1 0.1 pad_maximum_fusion
  53.3 2.9 %fusion.37 = f32[16,8,1,64]{3,2,1,0:T(1,128)S(1)} fusion(f32[16,8,64,1]{2,3,1,0:T(1,128)S(1)} %bitcast.91, f32[16,8,64,64]{3,2,1,0:T(8,128)} %param.22), kind=kOutput, calls=%fused_computation.108 | convolution fusion | flops 1048576 | bytes 2162688 | tf_op jit(solution)/shard_map/shd,shde->she/dot_general | solution.py:96
  56.2 0.2 multiply_reduce_fusion.1
  56.4 0.1 broadcast_multiply_fusion
  56.7 6.8 %all_to_all.30 = bf16[4,16,512]{2,1,0:T(8,128)(2,1)S(1)} all-to-all(bf16[4,16,512]{2,1,0:T(8,128)(2,1)S(1)} %broadcast_in_dim.28), channel_id=1, replica_groups=mesh['ep_0'=8,'ep_1'=4,'ep_2'=4,'tp'=2] {'ep_1'}, dimensions={0} | all-to-all | bytes 131072 | tf_op jit(solution)/shard_map/all_to_all | solution.py:20
  63.6 0.3 convolution_convert_fusion.3
  63.9 13.5 %all_to_all.31 = bf16[8,16,512]{2,1,0:T(8,128)(2,1)S(1)} all-to-all(bf16[8,16,512]{2,1,0:T(8,128)(2,1)S(1)} %bitcast.94), channel_id=1, replica_groups=mesh['ep_0'=8,'ep_1'=4,'ep_2'=4,'tp'=2] {'ep_1','tp'}, dimensions={0} | all-to-all | bytes 262144 | tf_op jit(solution)/shard_map/all_to_all | solution.py:20
  77.4 0.2 reshape.226
  77.6 0.1 copy.38
  77.7 0.2 reshape.227
  77.9 0.1 fusion.14
  78.1 0.1 fusion.13
  78.2 0.1 fusion.16
  78.3 0.1 fusion.18
  78.4 0.3 convolution_convert_fusion
  78.8 0.9 collective-permute-start.9
  79.7 0.1 collective-permute-start.10
  79.8 0.4 collective-permute-start.11
  80.2 1.2 reshape.228
  81.4 8.1 %all-to-all-start.4 = ((bf16[128,2,1024]{2,1,0:T(2,128)(2,1)}), bf16[128,2,1024]{2,1,0:T(2,128)(2,1)S(1)}, u32[]{:S(2)}, u32[]{:S(2)}) async-start(bf16[128,2,1024]{2,1,0:T(2,128)(2,1)} %reshape.228), calls=%async_computation.4 | async-start | bytes 1048576 | tf_op jit(solution)/shard_map/all_to_all | solution.py:20
  89.5 1.5 %fusion.38 = f32[16,256]{1,0:T(8,128)S(1)} fusion(bf16[16,2048]{1,0:T(8,128)(2,1)S(1)} %fusion.18, bf16[2048,256]{1,0:T(8,128)(2,1)} %param.37), kind=kOutput, calls=%fused_computation.109 | convolution fusion | flops 16777216 | bytes 1130496 | tf_op jit(solution)/shard_map/dot_general | solution.py:281
  90.9 2.0 %convolution_convert_fusion.1 = bf16[16,2048]{1,0:T(8,128)(2,1)S(1)} fusion(bf16[256,2048]{1,0:T(8,128)(2,1)S(1)} %copy-done, bf16[16,2048]{1,0:T(8,128)(2,1)S(1)} %fusion.18, bf16[2048,256]{1,0:T(8,128)(2,1)} %param.38, f32[16,256]{1,0:T(8,128)S(1)} %fusion.38), kind=kOutput, calls=%fused_computation.3 | convolution fusion | flops 33611776 | bytes 2244608 | tf_op jit(solution)/shard_map/dot_general | solution.py:284
  92.9 4.3 %multiply_add_fusion = f32[16,8,64,64]{3,2,1,0:T(8,128)} fusion(f32[16,8,64,64]{3,2,1,0:T(8,128)} %param.22, f32[16,8,64]{2,1,0:T(8,128)S(1)} %reshape.235, f32[16,8,64]{2,1,0:T(8,128)S(1)} %get-tuple-element.76, f32[8]{0:T(128)S(1)} %dynamic_slice.25), kind=kLoop, calls=%fused_computation.1 | loop fusion | flops 1572864 | bytes 4259872 | tf_op jit(solution)/shard_map/add | solution.py:108
  97.2 11.4 %all-to-all-done.4 = bf16[128,2,1024]{2,1,0:T(2,128)(2,1)S(1)} async-done(((bf16[128,2,1024]{2,1,0:T(2,128)(2,1)}), bf16[128,2,1024]{2,1,0:T(2,128)(2,1)S(1)}, u32[]{:S(2)}, u32[]{:S(2)}) %all-to-all-start.4) | async-done | bytes 524320 | tf_op jit(solution)/shard_map/all_to_all | solution.py:20
  108.5 0.1 copy.41
  108.7 3.5 %shard_map.204 = bf16[128,2048]{1,0:T(8,128)(2,1)S(1)} custom-call(bf16[128,2048]{1,0:T(8,128)(2,1)S(1)} %bitcast.78, bf16[2048,256]{1,0:T(8,128)(2,1)} %bitcast.82, bf16[2048,256]{1,0:T(8,128)(2,1)} %bitcast.85, bf16[2048,256]{1,0:T(8,128)(2,1)} %collective-permute-done.9.refs_2_, bf16[2048,256]{1,0:T(8,128)(2,1)} %collective-permute-done.10.refs_3_, ...), custom_call_target="tpu_custom_call" | custom-call | tf_op jit(solution)/shard_map/pallas_call | solution.py:140
  112.2 0.4 reshape.230
  112.5 24.1 %all_to_all.32 = bf16[128,2,1024]{2,1,0:T(2,128)(2,1)S(1)} all-to-all(bf16[128,2,1024]{2,1,0:T(2,128)(2,1)S(1)} %reshape.230), channel_id=1, replica_groups=mesh['ep_0'=8,'ep_1'=4,'ep_2'=4,'tp'=2] {'ep_0','ep_1','ep_2'}, dimensions={0} | all-to-all | bytes 1048576 | tf_op jit(solution)/shard_map/all_to_all | solution.py:20
  136.6 0.1 copy.42
  136.8 0.2 fusion.39
  137.0 4.0 %collective-permute-start.12 = (f32[16,2048]{1,0:T(8,128)S(1)}, f32[16,2048]{1,0:T(8,128)S(1)}, u32[]{:S(2)}, u32[]{:S(2)}) collective-permute-start(f32[16,2048]{1,0:T(8,128)S(1)} %convert_add_fusion.2), channel_id=1, source_target_pairs={{0,1},{1,0},{2,3},{3,2},{4,5},{5,4},{6,7},{7,6},{8,9},{9,8},{10,11... | collective-permute-start | bytes 393224 | tf_op jit(solution)/shard_map/ppermute | solution.py:28
  140.9 1.0 collective-permute-done.12
  141.9 0.1 multiply_reduce_fusion
  142.1 0.7 fusion.19
  (75 shorter events, 1.2 us)
Async XLA Ops:
  0.6 90.3 %copy-start = (bf16[256,2048]{1,0:T(8,128)(2,1)S(1)}, bf16[256,2048]{1,0:T(8,128)(2,1)}, u32[]{:S(2)}) copy-start(bf16[256,2048]{1,0:T(8,128)(2,1)} %param.39) | copy-start | bytes 3145732
  0.6 45.0 %copy-start.7 = (f32[16,6]{0,1:T(8,128)S(1)}, f32[16,6]{0,1:T(8,128)}, u32[]{:S(2)}) copy-start(f32[16,6]{0,1:T(8,128)} %param.33) | copy-start | bytes 1156
  0.7 39.7 %copy-start.6 = (s32[16,6]{0,1:T(8,128)S(1)}, s32[16,6]{0,1:T(8,128)}, u32[]{:S(2)}) copy-start(s32[16,6]{0,1:T(8,128)} %param.32) | copy-start | bytes 1156
  0.7 45.2 %copy-start.8 = (s32[16]{0:T(128)S(1)}, s32[16]{0:T(128)}, u32[]{:S(2)}) copy-start(s32[16]{0:T(128)} %param.21) | copy-start | bytes 196
  4.2 30.7 %all-to-all-start = ((bf16[32,16,640]{2,1,0:T(8,128)(2,1)}), bf16[32,16,640]{2,1,0:T(8,128)(2,1)S(1)}, u32[]{:S(2)}, u32[]{:S(2)}) async-start(bf16[32,16,640]{2,1,0:T(8,128)(2,1)} %get-tuple-element.29), calls=%async_computation | async-start | bytes 1310720 | tf_op jit(solution)/shard_map/all_to_all | solution.py:20
  17.4 6.9 %collective-permute-start.2 = (bf16[16,512]{1,0:T(8,128)(2,1)S(1)}, bf16[16,512]{1,0:T(8,128)(2,1)S(1)}, u32[]{:S(2)}, u32[]{:S(2)}) collective-permute-start(bf16[16,512]{1,0:T(8,128)(2,1)S(1)} %get-tuple-element.65), channel_id=1, source_target_pairs={{24,0},{0,8},{8,16},{16,24},{25,1},{1,9},{9,17},{17,25},{26,2},{2,... | collective-permute-start | bytes 49160 | tf_op jit(solution)/shard_map/ppermute | solution.py:38
  18.7 5.5 %collective-permute-start.1 = (bf16[16,512]{1,0:T(8,128)(2,1)S(1)}, bf16[16,512]{1,0:T(8,128)(2,1)S(1)}, u32[]{:S(2)}, u32[]{:S(2)}) collective-permute-start(bf16[16,512]{1,0:T(8,128)(2,1)S(1)} %get-tuple-element.67), channel_id=1, source_target_pairs={{16,0},{24,8},{0,16},{8,24},{17,1},{25,9},{1,17},{9,25},{18,2},{26... | collective-permute-start | bytes 49160 | tf_op jit(solution)/shard_map/ppermute | solution.py:38
  21.4 2.9 %collective-permute-start = (bf16[16,512]{1,0:T(8,128)(2,1)S(1)}, bf16[16,512]{1,0:T(8,128)(2,1)S(1)}, u32[]{:S(2)}, u32[]{:S(2)}) collective-permute-start(bf16[16,512]{1,0:T(8,128)(2,1)S(1)} %get-tuple-element.68), channel_id=1, source_target_pairs={{8,0},{16,8},{24,16},{0,24},{9,1},{17,9},{25,17},{1,25},{10,2},{18... | collective-permute-start | bytes 49160 | tf_op jit(solution)/shard_map/ppermute | solution.py:38
  24.3 4.3 %collective-permute-start.3 = (bf16[4,16,512]{2,1,0:T(8,128)(2,1)S(1)}, bf16[4,16,512]{2,1,0:T(8,128)(2,1)S(1)}, u32[]{:S(2)}, u32[]{:S(2)}) collective-permute-start(bf16[4,16,512]{2,1,0:T(8,128)(2,1)S(1)} %get-tuple-element.57), channel_id=1, source_target_pairs={{2,0},{4,2},{6,4},{0,6},{3,1},{5,3},{7,5},{1,7},{10,8},{12,10},{14... | collective-permute-start | bytes 196616 | tf_op jit(solution)/shard_map/ppermute | solution.py:38
  26.9 5.7 %collective-permute-start.5 = (bf16[4,16,512]{2,1,0:T(8,128)(2,1)S(1)}, bf16[4,16,512]{2,1,0:T(8,128)(2,1)S(1)}, u32[]{:S(2)}, u32[]{:S(2)}) collective-permute-start(bf16[4,16,512]{2,1,0:T(8,128)(2,1)S(1)} %get-tuple-element.57), channel_id=1, source_target_pairs={{6,0},{0,2},{2,4},{4,6},{7,1},{1,3},{3,5},{5,7},{14,8},{8,10},{10,... | collective-permute-start | bytes 196616 | tf_op jit(solution)/shard_map/ppermute | solution.py:38
  26.9 5.6 %collective-permute-start.4 = (bf16[4,16,512]{2,1,0:T(8,128)(2,1)S(1)}, bf16[4,16,512]{2,1,0:T(8,128)(2,1)S(1)}, u32[]{:S(2)}, u32[]{:S(2)}) collective-permute-start(bf16[4,16,512]{2,1,0:T(8,128)(2,1)S(1)} %get-tuple-element.57), channel_id=1, source_target_pairs={{4,0},{6,2},{0,4},{2,6},{5,1},{7,3},{1,5},{3,7},{12,8},{14,10},{8,... | collective-permute-start | bytes 196616 | tf_op jit(solution)/shard_map/ppermute | solution.py:38
  34.9 21.8 %collective-permute-start.8 = (bf16[512,128]{1,0:T(8,128)(2,1)S(1)}, bf16[512,128]{1,0:T(8,128)(2,1)S(1)}, u32[]{:S(2)}, u32[]{:S(2)}) collective-permute-start(bf16[512,128]{1,0:T(8,128)(2,1)S(1)} %slice.29), channel_id=1, source_target_pairs={{6,0},{0,2},{2,4},{4,6},{7,1},{1,3},{3,5},{5,7},{14,8},{8,10},{10,... | collective-permute-start | bytes 393224 | tf_op jit(solution)/shard_map/ppermute | solution.py:38
  35.8 20.9 %collective-permute-start.7 = (bf16[512,128]{1,0:T(8,128)(2,1)S(1)}, bf16[512,128]{1,0:T(8,128)(2,1)S(1)}, u32[]{:S(2)}, u32[]{:S(2)}) collective-permute-start(bf16[512,128]{1,0:T(8,128)(2,1)S(1)} %slice.29), channel_id=1, source_target_pairs={{4,0},{6,2},{0,4},{2,6},{5,1},{7,3},{1,5},{3,7},{12,8},{14,10},{8,... | collective-permute-start | bytes 393224 | tf_op jit(solution)/shard_map/ppermute | solution.py:38
  38.4 18.3 %collective-permute-start.6 = (bf16[512,128]{1,0:T(8,128)(2,1)S(1)}, bf16[512,128]{1,0:T(8,128)(2,1)S(1)}, u32[]{:S(2)}, u32[]{:S(2)}) collective-permute-start(bf16[512,128]{1,0:T(8,128)(2,1)S(1)} %slice.29), channel_id=1, source_target_pairs={{2,0},{4,2},{6,4},{0,6},{3,1},{5,3},{7,5},{1,7},{10,8},{12,10},{14... | collective-permute-start | bytes 393224 | tf_op jit(solution)/shard_map/ppermute | solution.py:38
  40.5 12.1 %all-to-all-start.1 = ((bf16[16,16,512]{2,1,0:T(8,128)(2,1)}), bf16[16,16,512]{2,1,0:T(8,128)(2,1)S(1)}, u32[]{:S(2)}, u32[]{:S(2)}) async-start(bf16[16,16,512]{2,1,0:T(8,128)(2,1)} %bitcast.15), calls=%async_computation.1 | async-start | bytes 524288 | tf_op jit(solution)/shard_map/all_to_all | solution.py:20
  53.2 24.9 %copy-start.2 = (bf16[16,2048]{1,0:T(8,128)(2,1)S(1)}, bf16[16,2048]{1,0:T(8,128)(2,1)}, u32[]{:S(2)}) copy-start(bf16[16,2048]{1,0:T(8,128)(2,1)} %tokens.1) | copy-start | bytes 196612
  53.2 24.9 %copy-start.3 = (f32[2048]{0:T(1024)S(1)}, f32[2048]{0:T(1024)}, u32[]{:S(2)}) copy-start(f32[2048]{0:T(1024)} %param.24) | copy-start | bytes 24580
  53.2 25.1 %copy-start.4 = (f32[2048]{0:T(1024)S(1)}, f32[2048]{0:T(1024)}, u32[]{:S(2)}) copy-start(f32[2048]{0:T(1024)} %param.25) | copy-start | bytes 24580
  53.2 25.5 %copy-start.1 = (bf16[1,2048,256]{2,1,0:T(8,128)(2,1)S(1)}, bf16[1,2048,256]{2,1,0:T(8,128)(2,1)}, u32[]{:S(2)}) copy-start(bf16[1,2048,256]{2,1,0:T(8,128)(2,1)} %param.34) | copy-start | bytes 3145732
  78.8 29.8 %collective-permute-start.9 = (bf16[2048,256]{1,0:T(8,128)(2,1)S(1)}, bf16[2048,256]{1,0:T(8,128)(2,1)}, u32[]{:S(2)}, u32[]{:S(2)}) collective-permute-start(bf16[2048,256]{1,0:T(8,128)(2,1)S(1)} %bitcast.83), channel_id=1, source_target_pairs={{0,1},{1,0},{2,3},{3,2},{4,5},{5,4},{6,7},{7,6},{8,9},{9,8},{10,11... | collective-permute-start | bytes 3145736 | tf_op jit(solution)/shard_map/ppermute | solution.py:28
  79.7 28.8 %collective-permute-start.10 = (bf16[2048,256]{1,0:T(8,128)(2,1)}, bf16[2048,256]{1,0:T(8,128)(2,1)}, u32[]{:S(2)}, u32[]{:S(2)}) collective-permute-start(bf16[2048,256]{1,0:T(8,128)(2,1)} %bitcast.84), channel_id=1, source_target_pairs={{0,1},{1,0},{2,3},{3,2},{4,5},{5,4},{6,7},{7,6},{8,9},{9,8},{10,11... | collective-permute-start | bytes 3145736 | tf_op jit(solution)/shard_map/ppermute | solution.py:28
  79.8 28.7 %collective-permute-start.11 = (bf16[256,2048]{1,0:T(8,128)(2,1)}, bf16[256,2048]{1,0:T(8,128)(2,1)}, u32[]{:S(2)}, u32[]{:S(2)}) collective-permute-start(bf16[256,2048]{1,0:T(8,128)(2,1)} %bitcast.86), channel_id=1, source_target_pairs={{0,1},{1,0},{2,3},{3,2},{4,5},{5,4},{6,7},{7,6},{8,9},{9,8},{10,11... | collective-permute-start | bytes 3145736 | tf_op jit(solution)/shard_map/ppermute | solution.py:28
  81.4 27.2 %all-to-all-start.4 = ((bf16[128,2,1024]{2,1,0:T(2,128)(2,1)}), bf16[128,2,1024]{2,1,0:T(2,128)(2,1)S(1)}, u32[]{:S(2)}, u32[]{:S(2)}) async-start(bf16[128,2,1024]{2,1,0:T(2,128)(2,1)} %reshape.228), calls=%async_computation.4 | async-start | bytes 1048576 | tf_op jit(solution)/shard_map/all_to_all | solution.py:20
  108.7 33.4 %copy-start.5 = (f32[2048]{0:T(1024)S(1)}, f32[2048]{0:T(1024)}, u32[]{:S(2)}) copy-start(f32[2048]{0:T(1024)} %param.26) | copy-start | bytes 24580
  137.0 5.0 %collective-permute-start.12 = (f32[16,2048]{1,0:T(8,128)S(1)}, f32[16,2048]{1,0:T(8,128)S(1)}, u32[]{:S(2)}, u32[]{:S(2)}) collective-permute-start(f32[16,2048]{1,0:T(8,128)S(1)} %convert_add_fusion.2), channel_id=1, source_target_pairs={{0,1},{1,0},{2,3},{3,2},{4,5},{5,4},{6,7},{7,6},{8,9},{9,8},{10,11... | collective-permute-start | bytes 393224 | tf_op jit(solution)/shard_map/ppermute | solution.py:28
